TPU v7x, 256 devices: a whole 4x4x8 slice. The times are simulated.
256 devices in a mesh: sp: 32 (over z, y), tp: 8 (over x, core).
Axes of the slice: x: 4, y: 4, z: 8, core: 2. Of those that a mesh axis runs over, the one named last changes fastest.
Arguments:
- residual: bfloat16 [16384, 2048], P(('sp', 'tp')), may hold values from -6 to 6
- query_major: bfloat16 [16384, 1024], P('sp', 'tp'), may hold values from -160 to 160
- keys_major: bfloat16 [16384, 1024], P('sp', 'tp'), may hold values from -6.5 to 6.5
- values_major: bfloat16 [16384, 1024], P('sp', 'tp'), may hold values from -6 to 6
- query_minor: bfloat16 [16384, 512], P('sp', 'tp'), may hold values from -160 to 160
- keys_minor: bfloat16 [16384, 512], P('sp', 'tp'), may hold values from -6.5 to 6.5
- values_minor: bfloat16 [16384, 512], P('sp', 'tp'), may hold values from -6 to 6
- lambda_major: float32 [8], P('tp'), may hold values from 0.3 to 0.8
- lambda_minor: float32 [8], P('tp'), may hold values from 0.3 to 0.8
- gain_major: float32 [128], replicated, may hold values from 0.1 to 1.9
- gain_minor: float32 [64], replicated, may hold values from 0.1 to 1.9
- output_major: bfloat16 [1024, 2048], P('tp'), may hold values from -0.15625 to 0.15625
- output_minor: bfloat16 [512, 2048], P('tp'), may hold values from -0.15625 to 0.15625
- mixer_gain: float32 [2048], replicated, may hold values from 0.1 to 1.9
- up_weight: bfloat16 [2048, 8192], P('sp', 'tp'), may hold values from -0.125 to 0.125
- down_weight: bfloat16 [8192, 2048], P('tp', 'sp'), may hold values from -0.0625 to 0.0625
Outputs:
- layer_out: bfloat16 [16384, 2048], P(('sp', 'tp'))
All inputs are finite; a program needn't handle non-finite values.
Results may differ from a plain program's by a relative error of at most 0.018.
Values may be sent and summed in bfloat16 or wider, within the bound.
No kernel may reach another device: no remote copies, remote signals or barrier semaphores. Data moves between devices by JAX's collectives and lax.ppermute only.
A program may use at most 128 MiB of HBM per device.

v0:
```python
import jax
import jax.numpy as jnp
from jax import lax
from jax.experimental import pallas as pl
from jax.experimental.pallas import tpu as pltpu
from jax.sharding import Mesh
from jax.sharding import PartitionSpec as P

DK_MAJOR = 64
DK_MINOR = 32
SEGMENT = 64
EPSILON = 1e-06
NEGATIVE = -1e30
LOG2E = 1.4426950408889634
SCALES = (DK_MAJOR**-0.5 * LOG2E,) * 2 + (DK_MINOR**-0.5 * LOG2E,) * 2
SP = ("z", "y")
TP = ("x", "c")
ROWS = 416
STATS = 384
NT = (((1,), (1,)), ((), ()))


def dot(a, b, dims=(((1,), (0,)), ((), ()))):
    return lax.dot_general(a, b, dims, preferred_element_type=jnp.float32)


def shifted(value, axis, by):
    size = lax.axis_size(axis)
    return lax.ppermute(value, axis, [(i, (i + by) % size) for i in range(size)])


def mirrored(value):
    size = lax.axis_size("z")
    return lax.ppermute(value, "z", [(i, size - 1 - i) for i in range(size)])


def attend_kernel(at_ref, q_ref, kv_ref, out_ref, vt_major, vt_minor, k_minor, accum, peak_ref):
    own_y, part, last = at_ref[0], at_ref[1], at_ref[2]
    pair = pl.program_id(0)
    length = vt_major.shape[2]
    half = length // 2

    @pl.when(pair == 0)
    def _():
        def turn(c, _):
            vt_major[c, :128] = kv_ref[c, :length, 128:256].T
            vt_major[c, 128:] = jnp.ones((16, length), jnp.bfloat16)
            for h in range(2):
                minor = kv_ref[c, length + h * 128 : length + (h + 1) * 128]
                vt_minor[c, :64, h * half : (h + 1) * half] = minor[64:]
                k_minor[c, h * half : (h + 1) * half] = minor.T
            vt_minor[c, 64:] = jnp.ones((16, length), jnp.bfloat16)
            return 0

        lax.fori_loop(0, last + 1, turn, 0)

    q = q_ref[...].reshape(length, q_ref.shape[2])
    lane = lax.broadcasted_iota(jnp.int32, (length, 128), 1)
    major = q[:, :128]
    minor = jnp.concatenate([q[:, 128:192], jnp.zeros((length, 64), q.dtype)], axis=1)
    zero = jnp.zeros_like(major)
    maps = (
        jnp.where(lane < 64, major, zero),
        jnp.where(lane >= 64, major, zero),
        jnp.where(lane < 32, minor, zero),
        jnp.where(lane >= 32, minor, zero),
    )
    accum[...] = jnp.zeros_like(accum)

    def fold(c, peaks, queries, columns, visible=None):
        scores = [dot(kv_ref[c, :length, :128] if m < 2 else k_minor[c], queries[m], NT) for m in range(4)]
        weights, factors, new = [], [], []
        for m in range(4):
            score = scores[m] if visible is None else jnp.where(visible, scores[m], NEGATIVE)
            peak = jnp.maximum(peaks[m], jnp.max(score, axis=0, keepdims=True))
            factors.append(jnp.exp2((peaks[m] - peak) * SCALES[m]))
            weights.append(jnp.exp2((score - peak) * SCALES[m]).astype(jnp.bfloat16))
            new.append(peak)
        for m in range(4):
            values = vt_major[c] if m < 2 else vt_minor[c]
            rows = values.shape[0]
            accum[m, :rows, columns] = accum[m, :rows, columns] * factors[m] + dot(values, weights[m])
        return tuple(new)

    start = tuple(jnp.full((1, length), NEGATIVE, jnp.float32) for _ in range(4))
    peaks = lax.fori_loop(0, last, lambda c, p: fold(c, p, maps, slice(None)), start)
    peak_ref[...] = jnp.concatenate(list(peaks), axis=0)

    for side in range(2):
        block_y = pair * 2 + side

        @pl.when(own_y <= block_y)
        def _(side=side, block_y=block_y):
            columns = slice(side * half, (side + 1) * half)
            key_at = own_y * length + lax.broadcasted_iota(jnp.int32, (length, 1), 0)
            query_at = block_y * length + part * half + lax.broadcasted_iota(jnp.int32, (1, half), 1)
            visible = key_at // SEGMENT <= query_at // SEGMENT
            old = tuple(peak_ref[m : m + 1, columns] for m in range(4))
            new = fold(last, old, [q_map[columns] for q_map in maps], columns, visible)
            peak_ref[:, columns] = jnp.concatenate(list(new), axis=0)

        columns = slice(side * half, (side + 1) * half)
        out_ref[side, 0:128] = accum[0, :128, columns].astype(jnp.bfloat16)
        out_ref[side, 128:256] = accum[1, :128, columns].astype(jnp.bfloat16)
        out_ref[side, 256:320] = accum[2, :64, columns].astype(jnp.bfloat16)
        out_ref[side, 320:384] = accum[3, :64, columns].astype(jnp.bfloat16)
        totals = [accum[0, 128:129, columns], accum[1, 128:129, columns], accum[2, 64:65, columns], accum[3, 64:65, columns]]
        stats = jnp.concatenate([peak_ref[:, columns]] + totals, axis=0)
        high = stats.astype(jnp.bfloat16).astype(jnp.float32)
        middle = (stats - high).astype(jnp.bfloat16).astype(jnp.float32)
        low = stats - high - middle
        parts = jnp.concatenate([high, middle, low, jnp.zeros_like(low)], axis=0)
        out_ref[side, STATS:] = parts.astype(jnp.bfloat16)


def attend(at, q, kv):
    blocks, length, width = q.shape
    chunks = kv.shape[0]
    return pl.pallas_call(
        attend_kernel,
        grid_spec=pltpu.PrefetchScalarGridSpec(
            num_scalar_prefetch=1,
            grid=(blocks // 2,),
            in_specs=[
                pl.BlockSpec((2, length // 2, width), lambda i, at: (i, at[1], 0)),
                pl.BlockSpec(kv.shape, lambda i, at: (0, 0, 0)),
            ],
            out_specs=pl.BlockSpec((2, ROWS, length // 2), lambda i, at: (i, 0, 0)),
            scratch_shapes=[
                pltpu.VMEM((chunks, 144, length), jnp.bfloat16),
                pltpu.VMEM((chunks, 80, length), jnp.bfloat16),
                pltpu.VMEM((chunks, length, 128), jnp.bfloat16),
                pltpu.VMEM((4, 144, length), jnp.float32),
                pltpu.VMEM((4, length), jnp.float32),
            ],
        ),
        out_shape=jax.ShapeDtypeStruct((blocks, ROWS, length // 2), jnp.bfloat16),
        compiler_params=pltpu.CompilerParams(vmem_limit_bytes=60 * 2**20),
        cost_estimate=pl.CostEstimate(flops=10**10, transcendentals=2 * 10**7, bytes_accessed=6 * 10**6),
    )(at, q, kv)


def merged(lam_ref, gain_major, gain_minor, part_ref):
    pieces = part_ref.shape[0]
    stats = []
    for p in range(pieces):
        coded = part_ref[p, STATS:].astype(jnp.float32)
        stats.append(coded[0:8] + coded[8:16] + coded[16:24])
    row = lax.broadcasted_iota(jnp.int32, (4, stats[0].shape[1]), 0)
    scale = jnp.where(row < 2, SCALES[0], SCALES[2])
    peak = stats[0][:4]
    for p in range(1, pieces):
        peak = jnp.maximum(peak, stats[p][:4])
    factors = [jnp.exp2((s[:4] - peak) * scale) for s in stats]
    total = factors[0] * stats[0][4:]
    for p in range(1, pieces):
        total = total + factors[p] * stats[p][4:]
    factors = [f / total for f in factors]

    def head(first, size, m, lam, gain):
        def summed(at, which):
            out = factors[0][which : which + 1] * part_ref[0, at : at + size].astype(jnp.float32)
            for p in range(1, pieces):
                out = out + factors[p][which : which + 1] * part_ref[p, at : at + size].astype(jnp.float32)
            return out

        diff = summed(first, m) - lam * summed(first + size, m + 1)
        mean = jnp.mean(diff * diff, axis=0, keepdims=True)
        return (diff * lax.rsqrt(mean + EPSILON) * gain).T

    major = head(0, 128, 0, lam_ref[0], gain_major[...])
    minor = head(256, 64, 2, lam_ref[1], gain_minor[...])
    rows = minor.shape[0] // 2
    minor = jnp.concatenate([minor[:rows], minor[rows:]], axis=1)
    return jnp.concatenate([major, minor], axis=0)


def merge_kernel(first_ref, lam_ref, gain_major, gain_minor, short_ref, long_ref, early_ref, late_ref):
    short = merged(lam_ref, gain_major, gain_minor, short_ref)
    long = merged(lam_ref, gain_major, gain_minor, long_ref)
    swap = first_ref[0] == 1
    early_ref[...] = jnp.where(swap, long, short).astype(jnp.bfloat16)
    late_ref[...] = jnp.where(swap, short, long).astype(jnp.bfloat16)


def merge(first, lams, gain_major, gain_minor, short, long):
    half = short.shape[2]
    whole = pl.BlockSpec(memory_space=pltpu.VMEM)
    scalars = pl.BlockSpec(memory_space=pltpu.SMEM)
    return pl.pallas_call(
        merge_kernel,
        in_specs=[scalars, scalars] + [whole] * 4,
        out_specs=[whole, whole],
        out_shape=[jax.ShapeDtypeStruct((half * 3 // 2, 128), jnp.bfloat16)] * 2,
        name="merge",
    )(first, lams, gain_major, gain_minor, short, long)


def mix_kernel(at_ref, heads0, heads1, gain_ref, *refs):
    fixed, (stream_ref, normed_ref, w, residual, x, stream, sems) = refs[:8], refs[8:]
    own_x, own_c = at_ref[0], at_ref[1]
    copies = []
    for i in range(8):
        side, d = divmod(i, 4)
        place = (own_x - d) % 4
        token = (place * 2 + (own_c + side) % 2) * 64
        piece = fixed[i]
        pairs = (
            (piece.at[pl.ds(0, 128)], w.at[pl.ds(i * 128, 128)]),
            (piece.at[pl.ds(128, 64)], w.at[pl.ds(1024 + i * 64, 64)]),
            (piece.at[pl.ds(192, 64)], residual.at[pl.ds(pl.multiple_of(token, 64), 64)]),
        )
        for k, (source, target) in enumerate(pairs):
            copies.append(pltpu.make_async_copy(source, target, sems.at[i, k]))
    for copy in copies:
        copy.start()
    for i in range(8):
        side, d = divmod(i, 4)
        heads = (heads0, heads1)[side]
        for h in range(2):
            at = h * 256
            x[at : at + 256, i * 128 : (i + 1) * 128] = heads[h * 4 + d, :256]
            columns = slice(1024 + i * 64, 1024 + (i + 1) * 64)
            x[at : at + 128, columns] = heads[h * 4 + d, 256:, :64]
            x[at + 128 : at + 256, columns] = heads[h * 4 + d, 256:, 64:]
    for copy in copies:
        copy.wait()
    for h in range(2):
        at = slice(h * 256, (h + 1) * 256)
        value = dot(x[at, :], w[...]) + residual[at, :].astype(jnp.float32)
        stream[at, :] = value
        mean = jnp.mean(value * value, axis=1, keepdims=True)
        normed_ref[at, :] = (value * lax.rsqrt(mean + EPSILON) * gain_ref[...]).astype(jnp.bfloat16)
    own = pl.ds(pl.multiple_of((own_x * 2 + own_c) * 64, 64), 64)
    stream_ref[...] = stream[own, :]


def mix(at, heads, fixed, gain):
    length, width = 512, fixed[0].shape[1]
    whole = pl.BlockSpec(memory_space=pltpu.VMEM)
    return pl.pallas_call(
        mix_kernel,
        in_specs=[pl.BlockSpec(memory_space=pltpu.SMEM)] + [whole] * 3 + [pl.BlockSpec(memory_space=pl.ANY)] * 8,
        out_specs=[whole, whole],
        out_shape=[
            jax.ShapeDtypeStruct((64, width), jnp.float32),
            jax.ShapeDtypeStruct((length, width), jnp.bfloat16),
        ],
        scratch_shapes=[
            pltpu.VMEM((1536, width), jnp.bfloat16),
            pltpu.VMEM((length, width), jnp.bfloat16),
            pltpu.VMEM((length, 1536), jnp.bfloat16),
            pltpu.VMEM((length, width), jnp.float32),
            pltpu.SemaphoreType.DMA((8, 3)),
        ],
        compiler_params=pltpu.CompilerParams(vmem_limit_bytes=60 * 2**20),
        cost_estimate=pl.CostEstimate(flops=33 * 10**8, transcendentals=0, bytes_accessed=12 * 10**6),
        name="mix",
    )(at, heads[0], heads[1], gain, *fixed)


def feed_kernel(at_ref, normed, weights, keep_ref, send_ref, up, down, hidden, sems):
    own_c, own_y = at_ref[1], at_ref[2]
    rows, width = normed.shape[1], up.shape[3]
    copies = [
        [
            pltpu.make_async_copy(
                weights.at[:, d, :, pl.ds(k * width, width)], target.at[:, (own_y - d) % 4], sems.at[k, d]
            )
            for d in range(4)
        ]
        for k, target in enumerate((up, down))
    ]
    for copy in copies[0] + copies[1]:
        copy.start()
    for copy in copies[0]:
        copy.wait()
    for h in range(2):
        value = jnp.maximum(dot(normed[h * 256 : (h + 1) * 256, :], up[...].reshape(rows, width)), 0.0)
        value = (value * value).astype(jnp.bfloat16)
        for k in range(4):
            x, c = h * 2 + k // 2, k % 2
            target = (own_c + c) % 2 * 256 + x * 64
            hidden[pl.ds(pl.multiple_of(target, 64), 64), :] = value[k * 64 : (k + 1) * 64]
    for copy in copies[1]:
        copy.wait()
    for side, ref in enumerate((keep_ref, send_ref)):
        out = dot(hidden[side * 256 : (side + 1) * 256, :], down[...].reshape(rows, width), NT)
        ref[...] = out.astype(jnp.bfloat16).reshape(ref.shape)


def feed(at, normed, weights):
    length, width = normed.shape
    whole = pl.BlockSpec(memory_space=pltpu.VMEM)
    shape = jax.ShapeDtypeStruct((4, 64, width), jnp.bfloat16)
    inner = weights.shape[3] // 2
    gathered = pltpu.VMEM(weights.shape[:3] + (inner,), jnp.bfloat16)
    return pl.pallas_call(
        feed_kernel,
        in_specs=[pl.BlockSpec(memory_space=pltpu.SMEM), whole, pl.BlockSpec(memory_space=pltpu.HBM)],
        out_specs=[whole, whole],
        out_shape=[shape, shape],
        scratch_shapes=[
            gathered,
            gathered,
            pltpu.VMEM((length, inner), jnp.bfloat16),
            pltpu.SemaphoreType.DMA((2, 4)),
        ],
        compiler_params=pltpu.CompilerParams(vmem_limit_bytes=60 * 2**20),
        cost_estimate=pl.CostEstimate(flops=44 * 10**8, transcendentals=0, bytes_accessed=14 * 10**6),
        name="feed",
    )(at, normed, weights)


def along(value, axis):
    return [value] + [shifted(value, axis, d) for d in (1, 2, 3)]


def body(
    residual,
    query_major,
    keys_major,
    values_major,
    query_minor,
    keys_minor,
    values_minor,
    lambda_major,
    lambda_minor,
    gain_major,
    gain_minor,
    output_major,
    output_minor,
    mixer_gain,
    up_weight,
    down_weight,
):
    z, y, x, c = (lax.axis_index(a) for a in ("z", "y", "x", "c"))
    minor = jnp.concatenate([keys_minor.T, values_minor.T], axis=0)
    kv = jnp.concatenate([keys_major, values_major], axis=1)
    kv = jnp.concatenate([kv, minor[:, :256], minor[:, 256:]], axis=0)
    kv = lax.all_gather(kv, "z")
    q = jnp.concatenate([query_major, query_minor], axis=1)
    half = q.shape[0] // 2
    q = jnp.concatenate([q[:half], mirrored(q[half:])], axis=0)
    fixed = jnp.concatenate([output_major, output_minor, residual], axis=0)
    fixed = along(fixed, "x")
    q = lax.all_gather(q, "y")
    weights = jnp.concatenate([up_weight, down_weight.T], axis=1)
    weights, q = lax.optimization_barrier((weights, q))
    weights = lax.all_gather(jnp.stack(along(weights, "y")), "z")

    mirror = lax.axis_size("z") - 1 - z
    short_part = (z > mirror).astype(jnp.int32)
    short = attend(jnp.stack([y, short_part, jnp.minimum(z, mirror)]), q, kv)
    short = lax.all_to_all(short, "y", 0, 0, tiled=True)
    long = attend(jnp.stack([y, 1 - short_part, jnp.maximum(z, mirror)]), q, kv)
    long, *fixed = lax.optimization_barrier((long, *fixed))
    fixed = fixed + [shifted(f, "c", 1) for f in fixed]
    long = lax.all_to_all(long, "y", 0, 0, tiled=True)
    lams = jnp.concatenate([lambda_major, lambda_minor])
    early, late = merge(short_part[None], lams, gain_major[:, None], gain_minor[:, None], short, long)
    heads = jnp.stack(along(early, "x") + along(mirrored(late), "x"))
    heads = (heads, shifted(heads, "c", 1))
    at = jnp.stack([x, c, y]).astype(jnp.int32)
    stream, normed = mix(at, heads, fixed, mixer_gain[None])
    keep, send = feed(at, normed, weights)
    pair = keep.astype(jnp.float32) + shifted(send, "c", 1).astype(jnp.float32)
    blocks = lax.all_to_all(pair.astype(jnp.bfloat16), "x", 0, 0, tiled=True)
    return (stream + jnp.sum(blocks.astype(jnp.float32), axis=0)).astype(jnp.bfloat16)


def solution(mesh):
    finer = Mesh(mesh.devices.reshape(8, 4, 4, 2), ("z", "y", "x", "c"))
    placed = (
        P(SP + TP, None),
        P(SP, TP),
        P(SP, TP),
        P(SP, TP),
        P(SP, TP),
        P(SP, TP),
        P(SP, TP),
        P(TP),
        P(TP),
        P(),
        P(),
        P(TP, None),
        P(TP, None),
        P(),
        P(SP, TP),
        P(TP, SP),
    )

    return jax.shard_map(body, mesh=finer, in_specs=placed, out_specs=P(SP + TP, None), check_vma=False)
```

profile of v0, /device:TPU:1, one launch (start us, length us, event | category | flops | bytes accessed | tf_op | source)
XLA Modules:
  0.0 211.0 jit_solution(4637146265087199429)
XLA Ops:
  6.5 0.8 fusion.2
  7.4 1.8 fusion
  9.2 1.0 copy.20
  10.2 0.9 fusion.1
  11.1 6.5 %collective-permute-start = (bf16[256,192]{1,0:T(8,128)(2,1)S(1)}, bf16[256,192]{1,0:T(8,128)(2,1)S(1)}, u32[]{:S(2)}, u32[]{:S(2)}) collective-permute-start(bf16[256,192]{1,0:T(8,128)(2,1)S(1)} %get-tuple-element.32), channel_id=1, source_target_pairs={{0,224},{32,192},{64,160},{96,128},{128,96},{160,64},{192,32},{224... | collective-permute-start | bytes 294920 | tf_op jit(solution)/shard_map/ppermute | solution.py:34
  17.6 6.3 %collective-permute-done = bf16[256,192]{1,0:T(8,128)(2,1)S(1)} collective-permute-done((bf16[256,192]{1,0:T(8,128)(2,1)S(1)}, bf16[256,192]{1,0:T(8,128)(2,1)S(1)}, u32[]{:S(2)}, u32[]{:S(2)}) %collective-permute-start) | collective-permute-done | bytes 98336 | tf_op jit(solution)/shard_map/ppermute | solution.py:34
  24.0 14.3 %all-gather = bf16[2048,192]{1,0:T(8,128)(2,1)} all-gather(bf16[512,192]{1,0:T(8,128)(2,1)S(1)} %pad_maximum_fusion.3), channel_id=2, replica_groups=mesh['z'=8,'y'=4,'x'=4,'c'=2] {'y'}, dimensions={0}, use_global_device_ids=true | all-gather | bytes 983040 | tf_op jit(solution)/shard_map/all_gather | solution.py:347
  38.2 1.2 collective-permute-start.18
  40.3 4.0 %collective-permute-done.18 = bf16[64,2048]{1,0:T(8,128)(2,1)S(1)} collective-permute-done((bf16[64,2048]{1,0:T(8,128)(2,1)S(1)}, bf16[64,2048]{1,0:T(8,128)(2,1)S(1)}, u32[]{:S(2)}, u32[]{:S(2)}) %collective-permute-start.18) | collective-permute-done | bytes 262176 | tf_op jit(solution)/shard_map/ppermute | solution.py:29
  44.3 2.0 collective-permute-done.17
  46.2 6.8 %collective-permute-done.16 = bf16[64,2048]{1,0:T(8,128)(2,1)S(1)} collective-permute-done((bf16[64,2048]{1,0:T(8,128)(2,1)S(1)}, bf16[64,2048]{1,0:T(8,128)(2,1)S(1)}, u32[]{:S(2)}, u32[]{:S(2)}) %collective-permute-start.16) | collective-permute-done | bytes 262176 | tf_op jit(solution)/shard_map/ppermute | solution.py:29
  53.0 1.2 pad_maximum_fusion
  54.3 1.3 collective-permute-start.1
  55.6 2.5 %collective-permute-start.2 = (bf16[256,2048]{1,0:T(8,128)(2,1)S(1)}, bf16[256,2048]{1,0:T(8,128)(2,1)}, u32[]{:S(2)}, u32[]{:S(2)}) collective-permute-start(bf16[256,2048]{1,0:T(8,128)(2,1)S(1)} %constant_dynamic-update-slice_fusion.refs_0_), channel_id=1, source_target_pairs={{0,4},{2,6},{4,0},{6,2},{1,5},{3,7},{5,1},{7,3},{8,12},{10,14},{12... | collective-permute-start | bytes 3145736 | tf_op jit(solution)/shard_map/ppermute | solution.py:29
  58.1 1.2 collective-permute-start.3
  60.4 8.4 %shard_map.154 = bf16[4,416,256]{2,1,0:T(8,128)(2,1)} custom-call(s32[3]{0:T(128)} %pad_add_fusion.1.at_ref, bf16[4,512,192]{2,1,0:T(8,128)(2,1)} %bitcast.36, bf16[8,768,256]{2,1,0:T(8,128)(2,1)} %bitcast.50), custom_call_target="tpu_custom_call" | custom-call | flops 10000000000 | bytes 6000000 | tf_op jit(solution)/shard_map/pallas_call | solution.py:119
  68.8 3.7 %all-to-all-start = ((bf16[4,416,256]{2,1,0:T(8,128)(2,1)}), bf16[4,416,256]{2,1,0:T(8,128)(2,1)S(1)}, u32[]{:S(2)}, u32[]{:S(2)}) async-start(bf16[4,416,256]{2,1,0:T(8,128)(2,1)} %shard_map.154), calls=%async_computation | async-start | bytes 1703936 | tf_op jit(solution)/shard_map/all_to_all | solution.py:355
  72.5 30.1 %shard_map.155 = bf16[4,416,256]{2,1,0:T(8,128)(2,1)} custom-call(s32[3]{0:T(128)} %pad_add_fusion.2.at_ref, bf16[4,512,192]{2,1,0:T(8,128)(2,1)} %bitcast.37, bf16[8,768,256]{2,1,0:T(8,128)(2,1)} %bitcast.51), custom_call_target="tpu_custom_call" | custom-call | flops 10000000000 | bytes 6000000 | tf_op jit(solution)/shard_map/pallas_call | solution.py:119
  102.8 3.5 %all-to-all-start.1 = ((bf16[4,416,256]{2,1,0:T(8,128)(2,1)}), bf16[4,416,256]{2,1,0:T(8,128)(2,1)S(1)}, u32[]{:S(2)}, u32[]{:S(2)}) async-start(bf16[4,416,256]{2,1,0:T(8,128)(2,1)} %shard_map.155), calls=%async_computation.1 | async-start | bytes 1703936 | tf_op jit(solution)/shard_map/all_to_all | solution.py:359
  107.6 0.7 copy.21.gain_major
  108.3 0.7 copy.22.gain_minor
  109.0 0.6 pad_maximum_fusion.5.lam_ref
  109.6 2.9 %collective-permute-start.12 = (bf16[256,2048]{1,0:T(8,128)(2,1)S(1)}, bf16[256,2048]{1,0:T(8,128)(2,1)}, u32[]{:S(2)}, u32[]{:S(2)}) collective-permute-start(bf16[256,2048]{1,0:T(8,128)(2,1)S(1)} %constant_dynamic-update-slice_fusion.refs_0_), channel_id=1, source_target_pairs={{0,1},{1,0},{2,3},{3,2},{4,5},{5,4},{6,7},{7,6},{8,9},{9,8},{10,11... | collective-permute-start | bytes 3145736 | tf_op jit(solution)/shard_map/ppermute | solution.py:29
  113.1 3.1 %all-to-all-done.1.long_ref = bf16[4,416,256]{2,1,0:T(8,128)(2,1)S(1)} async-done(((bf16[4,416,256]{2,1,0:T(8,128)(2,1)}), bf16[4,416,256]{2,1,0:T(8,128)(2,1)S(1)}, u32[]{:S(2)}, u32[]{:S(2)}) %all-to-all-start.1) | async-done | bytes 852000 | tf_op jit(solution)/shard_map/all_to_all | solution.py:359
  116.1 0.9 copy-done.1
  117.1 2.8 %merge.1 = (bf16[384,128]{1,0:T(8,128)(2,1)}, bf16[384,128]{1,0:T(8,128)(2,1)}) custom-call(s32[1]{0:T(128)} %bitcast.3.first_ref, f32[2]{0:T(128)} %pad_maximum_fusion.5.lam_ref, f32[128,1]{1,0:T(8,128)} %copy.21.gain_major, f32[64,1]{1,0:T(8,128)} %copy.22.gain_minor, bf16[4,416,256]{2,1,0:T(8,128)(2,1)} %copy-done, bf16[4,416,256]{2,1,0:T(8,128)(2,1)} %copy-done.1), custom_call_target="tpu_custom_call" | custom-call | tf_op jit(solution)/shard_map/merge/pallas_call | solution.py:190
  119.9 3.8 %collective-permute-start.4 = (bf16[384,128]{1,0:T(8,128)(2,1)}, bf16[384,128]{1,0:T(8,128)(2,1)S(1)}, u32[]{:S(2)}, u32[]{:S(2)}) collective-permute-start(bf16[384,128]{1,0:T(8,128)(2,1)} %get-tuple-element.20), channel_id=1, source_target_pairs={{0,2},{2,4},{4,6},{6,0},{1,3},{3,5},{5,7},{7,1},{8,10},{10,12},{12... | collective-permute-start | bytes 294920 | tf_op jit(solution)/shard_map/ppermute | solution.py:29
  123.7 0.9 bitcast_dynamic-update-slice_fusion.7
  124.6 3.6 %collective-permute-start.5 = (bf16[384,128]{1,0:T(8,128)(2,1)}, bf16[384,128]{1,0:T(8,128)(2,1)S(1)}, u32[]{:S(2)}, u32[]{:S(2)}) collective-permute-start(bf16[384,128]{1,0:T(8,128)(2,1)} %get-tuple-element.20), channel_id=1, source_target_pairs={{0,4},{2,6},{4,0},{6,2},{1,5},{3,7},{5,1},{7,3},{8,12},{10,14},{12... | collective-permute-start | bytes 294920 | tf_op jit(solution)/shard_map/ppermute | solution.py:29
  128.7 1.5 collective-permute-start.6
  130.2 0.7 collective-permute-done.5
  130.9 2.2 %collective-permute-done.6 = bf16[384,128]{1,0:T(8,128)(2,1)S(1)} collective-permute-done((bf16[384,128]{1,0:T(8,128)(2,1)}, bf16[384,128]{1,0:T(8,128)(2,1)S(1)}, u32[]{:S(2)}, u32[]{:S(2)}) %collective-permute-start.6) | collective-permute-done | bytes 98336 | tf_op jit(solution)/shard_map/ppermute | solution.py:29
  133.1 3.3 %collective-permute-start.15 = (bf16[256,2048]{1,0:T(8,128)(2,1)}, bf16[256,2048]{1,0:T(8,128)(2,1)}, u32[]{:S(2)}, u32[]{:S(2)}) collective-permute-start(bf16[256,2048]{1,0:T(8,128)(2,1)} %collective-permute-done.3.refs_3_), channel_id=1, source_target_pairs={{0,1},{1,0},{2,3},{3,2},{4,5},{5,4},{6,7},{7,6},{8,9},{9,8},{10,11... | collective-permute-start | bytes 3145736 | tf_op jit(solution)/shard_map/ppermute | solution.py:29
  136.4 3.4 %collective-permute-done.7 = bf16[384,128]{1,0:T(8,128)(2,1)S(1)} collective-permute-done((bf16[384,128]{1,0:T(8,128)(2,1)}, bf16[384,128]{1,0:T(8,128)(2,1)S(1)}, u32[]{:S(2)}, u32[]{:S(2)}) %collective-permute-start.7) | collective-permute-done | bytes 98336 | tf_op jit(solution)/shard_map/ppermute | solution.py:34
  139.9 5.0 %collective-permute-done.8 = bf16[384,128]{1,0:T(8,128)(2,1)S(1)} collective-permute-done((bf16[384,128]{1,0:T(8,128)(2,1)S(1)}, bf16[384,128]{1,0:T(8,128)(2,1)S(1)}, u32[]{:S(2)}, u32[]{:S(2)}) %collective-permute-start.8) | collective-permute-done | bytes 98336 | tf_op jit(solution)/shard_map/ppermute | solution.py:29
  144.9 1.5 collective-permute-start.9
  146.5 3.5 %collective-permute-done.9 = bf16[384,128]{1,0:T(8,128)(2,1)S(1)} collective-permute-done((bf16[384,128]{1,0:T(8,128)(2,1)S(1)}, bf16[384,128]{1,0:T(8,128)(2,1)S(1)}, u32[]{:S(2)}, u32[]{:S(2)}) %collective-permute-start.9) | collective-permute-done | bytes 98336 | tf_op jit(solution)/shard_map/ppermute | solution.py:29
  150.3 3.5 %collective-permute-done.10 = bf16[384,128]{1,0:T(8,128)(2,1)S(1)} collective-permute-done((bf16[384,128]{1,0:T(8,128)(2,1)S(1)}, bf16[384,128]{1,0:T(8,128)(2,1)S(1)}, u32[]{:S(2)}, u32[]{:S(2)}) %collective-permute-start.10) | collective-permute-done | bytes 98336 | tf_op jit(solution)/shard_map/ppermute | solution.py:29
  153.9 5.0 %collective-permute-start.11 = (bf16[8,384,128]{2,1,0:T(8,128)(2,1)S(1)}, bf16[8,384,128]{2,1,0:T(8,128)(2,1)S(1)}, u32[]{:S(2)}, u32[]{:S(2)}) collective-permute-start(bf16[8,384,128]{2,1,0:T(8,128)(2,1)S(1)} %bitcast_dynamic-update-slice_fusion.heads0), channel_id=1, source_target_pairs={{0,1},{1,0},{2,3},{3,2},{4,5},{5,4},{6,7},{7,6},{8,9},{9,8},{10,11... | collective-permute-start | bytes 2359304 | tf_op jit(solution)/shard_map/ppermute | solution.py:29
  158.9 0.7 pad_add_fusion.at_ref
  159.6 1.2 collective-permute-done.11.heads1
  160.8 0.9 copy-done.12
  161.7 10.2 %mix.1 = (f32[64,2048]{1,0:T(8,128)}, bf16[512,2048]{1,0:T(8,128)(2,1)}) custom-call(s32[3]{0:T(128)} %pad_add_fusion.at_ref, bf16[8,384,128]{2,1,0:T(8,128)(2,1)} %copy-done.9, bf16[8,384,128]{2,1,0:T(8,128)(2,1)} %copy-done.12, f32[1,2048]{1,0:T(1,128)} %bitcast.52, bf16[256,2048]{1,0:T(8,128)(2,1)} %copy-done.4, ...), custom_call_target="tpu_custom_call" | custom-call | flops 3300000000 | bytes 12000000 | tf_op jit(solution)/shard_map/mix/pallas_call | solution.py:241
  171.9 9.6 %feed.1 = (bf16[4,64,2048]{2,1,0:T(8,128)(2,1)}, bf16[4,64,2048]{2,1,0:T(8,128)(2,1)}) custom-call(s32[3]{0:T(128)} %pad_add_fusion.at_ref, bf16[512,2048]{1,0:T(8,128)(2,1)} %get-tuple-element.27.normed, bf16[8,4,64,2048]{3,2,1,0:T(8,128)(2,1)} %bitcast.49), custom_call_target="tpu_custom_call" | custom-call | flops 4400000000 | bytes 14000000 | tf_op jit(solution)/shard_map/feed/pallas_call | solution.py:298
  182.0 2.5 %collective-permute-done.19 = bf16[4,64,2048]{2,1,0:T(8,128)(2,1)S(1)} collective-permute-done((bf16[4,64,2048]{2,1,0:T(8,128)(2,1)}, bf16[4,64,2048]{2,1,0:T(8,128)(2,1)S(1)}, u32[]{:S(2)}, u32[]{:S(2)}) %collective-permute-start.19) | collective-permute-done | bytes 1048608 | tf_op jit(solution)/shard_map/ppermute | solution.py:29
  184.5 1.6 add_convert_fusion
  186.1 17.2 %all_to_all.15 = bf16[4,64,2048]{2,1,0:T(8,128)(2,1)S(1)} all-to-all(bf16[4,64,2048]{2,1,0:T(8,128)(2,1)S(1)} %add_convert_fusion), channel_id=1, replica_groups=mesh['z'=8,'y'=4,'x'=4,'c'=2] {'x'}, dimensions={0} | all-to-all | bytes 2097152 | tf_op jit(solution)/shard_map/all_to_all | solution.py:368
  203.4 0.8 add_convert_fusion.1
  (62 shorter events, 4.6 us)
Async XLA Ops:
  6.5 11.1 %copy-start.7 = (bf16[1024,64]{0,1:T(8,128)(2,1)S(1)}, bf16[1024,64]{0,1:T(8,128)(2,1)}, u32[]{:S(2)}) copy-start(bf16[1024,64]{0,1:T(8,128)(2,1)} %param.31) | copy-start | bytes 393220
  6.5 11.1 %copy-start.8 = (bf16[64,1024]{1,0:T(8,128)(2,1)S(1)}, bf16[64,1024]{1,0:T(8,128)(2,1)}, u32[]{:S(2)}) copy-start(bf16[64,1024]{1,0:T(8,128)(2,1)} %param.30) | copy-start | bytes 393220
  6.5 53.9 %all-gather.6.cloned.1.call-start = ((), (), s32[]{:S(2)}) async-start(), calls=%async_computation.3 | async-start | bytes 3538944 | tf_op jit(solution)/shard_map/all_gather | solution.py:341
  9.2 162.7 %all-gather.8.cloned.1.call-start = ((), (), s32[]{:S(2)}) async-start(), calls=%async_computation.4 | async-start | bytes 9437184 | tf_op jit(solution)/shard_map/all_gather | solution.py:350
  11.1 12.8 %collective-permute-start = (bf16[256,192]{1,0:T(8,128)(2,1)S(1)}, bf16[256,192]{1,0:T(8,128)(2,1)S(1)}, u32[]{:S(2)}, u32[]{:S(2)}) collective-permute-start(bf16[256,192]{1,0:T(8,128)(2,1)S(1)} %get-tuple-element.32), channel_id=1, source_target_pairs={{0,224},{32,192},{64,160},{96,128},{128,96},{160,64},{192,32},{224... | collective-permute-start | bytes 294920 | tf_op jit(solution)/shard_map/ppermute | solution.py:34
  24.0 30.2 %copy-start.2 = (bf16[128,2048]{1,0:T(8,128)(2,1)S(1)}, bf16[128,2048]{1,0:T(8,128)(2,1)}, u32[]{:S(2)}) copy-start(bf16[128,2048]{1,0:T(8,128)(2,1)} %param.27) | copy-start | bytes 1572868
  38.2 6.0 %collective-permute-start.18 = (bf16[64,2048]{1,0:T(8,128)(2,1)S(1)}, bf16[64,2048]{1,0:T(8,128)(2,1)S(1)}, u32[]{:S(2)}, u32[]{:S(2)}) collective-permute-start(bf16[64,2048]{1,0:T(8,128)(2,1)S(1)} %pad_maximum_fusion.2), channel_id=1, source_target_pairs={{0,24},{8,0},{16,8},{24,16},{1,25},{9,1},{17,9},{25,17},{2,26},{10... | collective-permute-start | bytes 786440 | tf_op jit(solution)/shard_map/ppermute | solution.py:29
  39.4 6.8 %collective-permute-start.17 = (bf16[64,2048]{1,0:T(8,128)(2,1)S(1)}, bf16[64,2048]{1,0:T(8,128)(2,1)S(1)}, u32[]{:S(2)}, u32[]{:S(2)}) collective-permute-start(bf16[64,2048]{1,0:T(8,128)(2,1)S(1)} %pad_maximum_fusion.2), channel_id=1, source_target_pairs={{0,16},{8,24},{16,0},{24,8},{1,17},{9,25},{17,1},{25,9},{2,18},{10... | collective-permute-start | bytes 786440 | tf_op jit(solution)/shard_map/ppermute | solution.py:29
  40.0 13.0 %collective-permute-start.16 = (bf16[64,2048]{1,0:T(8,128)(2,1)S(1)}, bf16[64,2048]{1,0:T(8,128)(2,1)S(1)}, u32[]{:S(2)}, u32[]{:S(2)}) collective-permute-start(bf16[64,2048]{1,0:T(8,128)(2,1)S(1)} %pad_maximum_fusion.2), channel_id=1, source_target_pairs={{0,8},{8,16},{16,24},{24,0},{1,9},{9,17},{17,25},{25,1},{2,10},{10... | collective-permute-start | bytes 786440 | tf_op jit(solution)/shard_map/ppermute | solution.py:29
  53.0 1.2 copy-start.5
  53.0 1.3 copy-start.6
  54.3 55.3 %copy-start.4 = (bf16[256,2048]{1,0:T(8,128)(2,1)}, bf16[256,2048]{1,0:T(8,128)(2,1)S(1)}, u32[]{:S(2)}) copy-start(bf16[256,2048]{1,0:T(8,128)(2,1)S(1)} %constant_dynamic-update-slice_fusion.refs_0_) | copy-start | bytes 3145732
  54.3 48.2 %collective-permute-start.1 = (bf16[256,2048]{1,0:T(8,128)(2,1)S(1)}, bf16[256,2048]{1,0:T(8,128)(2,1)}, u32[]{:S(2)}, u32[]{:S(2)}) collective-permute-start(bf16[256,2048]{1,0:T(8,128)(2,1)S(1)} %constant_dynamic-update-slice_fusion.refs_0_), channel_id=1, source_target_pairs={{0,2},{2,4},{4,6},{6,0},{1,3},{3,5},{5,7},{7,1},{8,10},{10,12},{12... | collective-permute-start | bytes 3145736 | tf_op jit(solution)/shard_map/ppermute | solution.py:29
  55.6 47.0 %collective-permute-start.2 = (bf16[256,2048]{1,0:T(8,128)(2,1)S(1)}, bf16[256,2048]{1,0:T(8,128)(2,1)}, u32[]{:S(2)}, u32[]{:S(2)}) collective-permute-start(bf16[256,2048]{1,0:T(8,128)(2,1)S(1)} %constant_dynamic-update-slice_fusion.refs_0_), channel_id=1, source_target_pairs={{0,4},{2,6},{4,0},{6,2},{1,5},{3,7},{5,1},{7,3},{8,12},{10,14},{12... | collective-permute-start | bytes 3145736 | tf_op jit(solution)/shard_map/ppermute | solution.py:29
  58.1 44.7 %collective-permute-start.3 = (bf16[256,2048]{1,0:T(8,128)(2,1)S(1)}, bf16[256,2048]{1,0:T(8,128)(2,1)}, u32[]{:S(2)}, u32[]{:S(2)}) collective-permute-start(bf16[256,2048]{1,0:T(8,128)(2,1)S(1)} %constant_dynamic-update-slice_fusion.refs_0_), channel_id=1, source_target_pairs={{0,6},{2,0},{4,2},{6,4},{1,7},{3,1},{5,3},{7,5},{8,14},{10,8},{12,... | collective-permute-start | bytes 3145736 | tf_op jit(solution)/shard_map/ppermute | solution.py:29
  68.8 34.0 %all-to-all-start = ((bf16[4,416,256]{2,1,0:T(8,128)(2,1)}), bf16[4,416,256]{2,1,0:T(8,128)(2,1)S(1)}, u32[]{:S(2)}, u32[]{:S(2)}) async-start(bf16[4,416,256]{2,1,0:T(8,128)(2,1)} %shard_map.154), calls=%async_computation | async-start | bytes 1703936 | tf_op jit(solution)/shard_map/all_to_all | solution.py:355
  72.5 35.1 %copy-start.10 = (f32[128]{0:T(128)S(1)}, f32[128]{0:T(128)}, u32[]{:S(2)}) copy-start(f32[128]{0:T(128)} %param.25) | copy-start | bytes 1540
  72.5 35.8 %copy-start.11 = (f32[64]{0:T(128)S(1)}, f32[64]{0:T(128)}, u32[]{:S(2)}) copy-start(f32[64]{0:T(128)} %param.26) | copy-start | bytes 772
  102.8 13.4 %copy-start = (bf16[4,416,256]{2,1,0:T(8,128)(2,1)}, bf16[4,416,256]{2,1,0:T(8,128)(2,1)S(1)}, u32[]{:S(2)}) copy-start(bf16[4,416,256]{2,1,0:T(8,128)(2,1)S(1)} %all-to-all-done.short_ref) | copy-start | bytes 2555908
  102.8 13.4 %all-to-all-start.1 = ((bf16[4,416,256]{2,1,0:T(8,128)(2,1)}), bf16[4,416,256]{2,1,0:T(8,128)(2,1)S(1)}, u32[]{:S(2)}, u32[]{:S(2)}) async-start(bf16[4,416,256]{2,1,0:T(8,128)(2,1)} %shard_map.155), calls=%async_computation.1 | async-start | bytes 1703936 | tf_op jit(solution)/shard_map/all_to_all | solution.py:359
  109.6 50.0 %collective-permute-start.12 = (bf16[256,2048]{1,0:T(8,128)(2,1)S(1)}, bf16[256,2048]{1,0:T(8,128)(2,1)}, u32[]{:S(2)}, u32[]{:S(2)}) collective-permute-start(bf16[256,2048]{1,0:T(8,128)(2,1)S(1)} %constant_dynamic-update-slice_fusion.refs_0_), channel_id=1, source_target_pairs={{0,1},{1,0},{2,3},{3,2},{4,5},{5,4},{6,7},{7,6},{8,9},{9,8},{10,11... | collective-permute-start | bytes 3145736 | tf_op jit(solution)/shard_map/ppermute | solution.py:29
  112.6 47.0 %collective-permute-start.13 = (bf16[256,2048]{1,0:T(8,128)(2,1)}, bf16[256,2048]{1,0:T(8,128)(2,1)}, u32[]{:S(2)}, u32[]{:S(2)}) collective-permute-start(bf16[256,2048]{1,0:T(8,128)(2,1)} %collective-permute-done.1.refs_1_), channel_id=1, source_target_pairs={{0,1},{1,0},{2,3},{3,2},{4,5},{5,4},{6,7},{7,6},{8,9},{9,8},{10,11... | collective-permute-start | bytes 3145736 | tf_op jit(solution)/shard_map/ppermute | solution.py:29
  112.6 47.0 %collective-permute-start.14 = (bf16[256,2048]{1,0:T(8,128)(2,1)}, bf16[256,2048]{1,0:T(8,128)(2,1)}, u32[]{:S(2)}, u32[]{:S(2)}) collective-permute-start(bf16[256,2048]{1,0:T(8,128)(2,1)} %collective-permute-done.2.refs_2_), channel_id=1, source_target_pairs={{0,1},{1,0},{2,3},{3,2},{4,5},{5,4},{6,7},{7,6},{8,9},{9,8},{10,11... | collective-permute-start | bytes 3145736 | tf_op jit(solution)/shard_map/ppermute | solution.py:29
  116.1 0.9 copy-start.1
  119.9 8.8 %collective-permute-start.4 = (bf16[384,128]{1,0:T(8,128)(2,1)}, bf16[384,128]{1,0:T(8,128)(2,1)S(1)}, u32[]{:S(2)}, u32[]{:S(2)}) collective-permute-start(bf16[384,128]{1,0:T(8,128)(2,1)} %get-tuple-element.20), channel_id=1, source_target_pairs={{0,2},{2,4},{4,6},{6,0},{1,3},{3,5},{5,7},{7,1},{8,10},{10,12},{12... | collective-permute-start | bytes 294920 | tf_op jit(solution)/shard_map/ppermute | solution.py:29
  124.6 6.3 %collective-permute-start.5 = (bf16[384,128]{1,0:T(8,128)(2,1)}, bf16[384,128]{1,0:T(8,128)(2,1)S(1)}, u32[]{:S(2)}, u32[]{:S(2)}) collective-permute-start(bf16[384,128]{1,0:T(8,128)(2,1)} %get-tuple-element.20), channel_id=1, source_target_pairs={{0,4},{2,6},{4,0},{6,2},{1,5},{3,7},{5,1},{7,3},{8,12},{10,14},{12... | collective-permute-start | bytes 294920 | tf_op jit(solution)/shard_map/ppermute | solution.py:29
  128.7 4.4 %collective-permute-start.6 = (bf16[384,128]{1,0:T(8,128)(2,1)}, bf16[384,128]{1,0:T(8,128)(2,1)S(1)}, u32[]{:S(2)}, u32[]{:S(2)}) collective-permute-start(bf16[384,128]{1,0:T(8,128)(2,1)} %get-tuple-element.20), channel_id=1, source_target_pairs={{0,6},{2,0},{4,2},{6,4},{1,7},{3,1},{5,3},{7,5},{8,14},{10,8},{12,... | collective-permute-start | bytes 294920 | tf_op jit(solution)/shard_map/ppermute | solution.py:29
  130.9 9.0 %collective-permute-start.7 = (bf16[384,128]{1,0:T(8,128)(2,1)}, bf16[384,128]{1,0:T(8,128)(2,1)S(1)}, u32[]{:S(2)}, u32[]{:S(2)}) collective-permute-start(bf16[384,128]{1,0:T(8,128)(2,1)} %get-tuple-element.21), channel_id=1, source_target_pairs={{0,224},{32,192},{64,160},{96,128},{128,96},{160,64},{192,32},{224... | collective-permute-start | bytes 294920 | tf_op jit(solution)/shard_map/ppermute | solution.py:34
  133.1 26.5 %collective-permute-start.15 = (bf16[256,2048]{1,0:T(8,128)(2,1)}, bf16[256,2048]{1,0:T(8,128)(2,1)}, u32[]{:S(2)}, u32[]{:S(2)}) collective-permute-start(bf16[256,2048]{1,0:T(8,128)(2,1)} %collective-permute-done.3.refs_3_), channel_id=1, source_target_pairs={{0,1},{1,0},{2,3},{3,2},{4,5},{5,4},{6,7},{7,6},{8,9},{9,8},{10,11... | collective-permute-start | bytes 3145736 | tf_op jit(solution)/shard_map/ppermute | solution.py:29
  139.9 5.1 %collective-permute-start.8 = (bf16[384,128]{1,0:T(8,128)(2,1)S(1)}, bf16[384,128]{1,0:T(8,128)(2,1)S(1)}, u32[]{:S(2)}, u32[]{:S(2)}) collective-permute-start(bf16[384,128]{1,0:T(8,128)(2,1)S(1)} %collective-permute-done.7), channel_id=1, source_target_pairs={{0,2},{2,4},{4,6},{6,0},{1,3},{3,5},{5,7},{7,1},{8,10},{10,12},{12... | collective-permute-start | bytes 294920 | tf_op jit(solution)/shard_map/ppermute | solution.py:29
  144.9 5.0 %collective-permute-start.9 = (bf16[384,128]{1,0:T(8,128)(2,1)S(1)}, bf16[384,128]{1,0:T(8,128)(2,1)S(1)}, u32[]{:S(2)}, u32[]{:S(2)}) collective-permute-start(bf16[384,128]{1,0:T(8,128)(2,1)S(1)} %collective-permute-done.7), channel_id=1, source_target_pairs={{0,4},{2,6},{4,0},{6,2},{1,5},{3,7},{5,1},{7,3},{8,12},{10,14},{12... | collective-permute-start | bytes 294920 | tf_op jit(solution)/shard_map/ppermute | solution.py:29
  150.0 3.9 %collective-permute-start.10 = (bf16[384,128]{1,0:T(8,128)(2,1)S(1)}, bf16[384,128]{1,0:T(8,128)(2,1)S(1)}, u32[]{:S(2)}, u32[]{:S(2)}) collective-permute-start(bf16[384,128]{1,0:T(8,128)(2,1)S(1)} %collective-permute-done.7), channel_id=1, source_target_pairs={{0,6},{2,0},{4,2},{6,4},{1,7},{3,1},{5,3},{7,5},{8,14},{10,8},{12,... | collective-permute-start | bytes 294920 | tf_op jit(solution)/shard_map/ppermute | solution.py:29
  153.8 7.0 %copy-start.9 = (bf16[8,384,128]{2,1,0:T(8,128)(2,1)}, bf16[8,384,128]{2,1,0:T(8,128)(2,1)S(1)}, u32[]{:S(2)}) copy-start(bf16[8,384,128]{2,1,0:T(8,128)(2,1)S(1)} %bitcast_dynamic-update-slice_fusion.heads0) | copy-start | bytes 2359300
  153.9 7.0 %collective-permute-start.11 = (bf16[8,384,128]{2,1,0:T(8,128)(2,1)S(1)}, bf16[8,384,128]{2,1,0:T(8,128)(2,1)S(1)}, u32[]{:S(2)}, u32[]{:S(2)}) collective-permute-start(bf16[8,384,128]{2,1,0:T(8,128)(2,1)S(1)} %bitcast_dynamic-update-slice_fusion.heads0), channel_id=1, source_target_pairs={{0,1},{1,0},{2,3},{3,2},{4,5},{5,4},{6,7},{7,6},{8,9},{9,8},{10,11... | collective-permute-start | bytes 2359304 | tf_op jit(solution)/shard_map/ppermute | solution.py:29
  160.8 0.9 copy-start.12
  181.5 3.0 %collective-permute-start.19 = (bf16[4,64,2048]{2,1,0:T(8,128)(2,1)}, bf16[4,64,2048]{2,1,0:T(8,128)(2,1)S(1)}, u32[]{:S(2)}, u32[]{:S(2)}) collective-permute-start(bf16[4,64,2048]{2,1,0:T(8,128)(2,1)} %get-tuple-element.30), channel_id=1, source_target_pairs={{0,1},{1,0},{2,3},{3,2},{4,5},{5,4},{6,7},{7,6},{8,9},{9,8},{10,11... | collective-permute-start | bytes 3145736 | tf_op jit(solution)/shard_map/ppermute | solution.py:29
  186.1 17.3 %copy-start.3 = (f32[64,2048]{1,0:T(8,128)S(1)}, f32[64,2048]{1,0:T(8,128)}, u32[]{:S(2)}) copy-start(f32[64,2048]{1,0:T(8,128)} %get-tuple-element.26) | copy-start | bytes 1572868
Sparse Core Ops, SparseCore 0:
  9.3 48.2 all-gather.5
  59.3 97.2 all-gather.7
where the time goes:
time: 212 us; the launch traced here: 211 us
  Pallas kernels  61.1 us (29%)
  waiting for transfers between devices  44.9 us (21%)
  starting transfers between devices  43.6 us (21%)
  blocking collectives  31.4 us (15%)
  between operations  15 us (7%)
  other arithmetic  9.71 us (5%)
  local copies, waits for them, and re-layouts  5.38 us (3%)
    pallas_call x2, Pallas kernels, attend(): pl.pallas_call(attend_kernel, grid_spec=pltpu.PrefetchScalarGridSpec(num_...  38.4 us
    ppermute x18, waiting for transfers between devices, shifted(): lax.ppermute(value, axis, [(i, (i + by) % size) for i in range(size)])  32 us
    ppermute x18, starting transfers between devices, shifted(): lax.ppermute(value, axis, [(i, (i + by) % size) for i in range(size)])  29.9 us
    all_to_all x1, blocking collectives, body(): blocks = lax.all_to_all(pair.astype(jnp.bfloat16), 'x', 0, 0, tiled=True)  17.2 us
    all_gather x1, blocking collectives, body(): q = lax.all_gather(q, 'y')  14.3 us
    pallas_call x1, Pallas kernels, mix(): pl.pallas_call(mix_kernel, in_specs=[pl.BlockSpec(memory_space=pltpu.SMEM...  10.2 us
    ppermute x2, waiting for transfers between devices, mirrored(): return lax.ppermute(value, 'z', [(i, size - 1 - i) for i in range(size)])  9.72 us
    pallas_call x1, Pallas kernels, feed(): pl.pallas_call(feed_kernel, in_specs=[pl.BlockSpec(memory_space=pltpu.SME...  9.6 us
  transfers between devices with their start and end apart: 24, of which 15 were waited for; matrix products, arithmetic and copies ran while one was open for 4% of the time, Pallas kernels for 24%

commit v1 on v0

--- a/solution.py
+++ b/solution.py
@@ -341,13 +341,14 @@
     kv = lax.all_gather(kv, "z")
     q = jnp.concatenate([query_major, query_minor], axis=1)
     half = q.shape[0] // 2
-    q = jnp.concatenate([q[:half], mirrored(q[half:])], axis=0)
+    late = mirrored(q[half:])
+    q = jnp.concatenate([q[:half], late], axis=0)
     fixed = jnp.concatenate([output_major, output_minor, residual], axis=0)
     fixed = along(fixed, "x")
     q = lax.all_gather(q, "y")
     weights = jnp.concatenate([up_weight, down_weight.T], axis=1)
-    weights, q = lax.optimization_barrier((weights, q))
-    weights = lax.all_gather(jnp.stack(along(weights, "y")), "z")
+    weights = along(weights, "y")
+    weights = lax.all_gather(jnp.stack(weights), "z")
 
     mirror = lax.axis_size("z") - 1 - z
     short_part = (z > mirror).astype(jnp.int32)

time: 212 us -> 215 us (1.014)
  starting transfers between devices: 43.6 us -> 55.2 us
  waiting for transfers between devices: 44.9 us -> 38.5 us
    ppermute x18, starting transfers between devices: 29.9 us -> 41.9 us  [shifted(): lax.ppermute(value, axis, [(i, (i + by) % size) for i in range(size)])]
    all_to_all x1, waiting for transfers between devices: 3.07 us -> 0.17 us  [body(): long = lax.all_to_all(long, 'y', 0, 0, tiled=True)]
    ppermute x18, waiting for transfers between devices: 32 us -> 29.5 us  [shifted(): lax.ppermute(value, axis, [(i, (i + by) % size) for i in range(size)])]
  transfers between devices with their start and end apart: 24 -> 24, of which waited for: 15 -> 13; matrix products, arithmetic and copies ran while one was open for 4% -> 3% of each run, Pallas kernels for 24% -> 24%
where the time goes in v1:
time: 215 us; the launch traced here: 214 us
  Pallas kernels  61.1 us (28%)
  starting transfers between devices  55.2 us (26%)
  waiting for transfers between devices  38.5 us (18%)
  blocking collectives  30.1 us (14%)
  between operations  15 us (7%)
  other arithmetic  9.88 us (5%)
  local copies, waits for them, and re-layouts  4.51 us (2%)
    ppermute x18, starting transfers between devices, shifted(): lax.ppermute(value, axis, [(i, (i + by) % size) for i in range(size)])  41.9 us
    pallas_call x2, Pallas kernels, attend(): pl.pallas_call(attend_kernel, grid_spec=pltpu.PrefetchScalarGridSpec(num_...  38.4 us
    ppermute x18, waiting for transfers between devices, shifted(): lax.ppermute(value, axis, [(i, (i + by) % size) for i in range(size)])  29.5 us
    all_to_all x1, blocking collectives, body(): blocks = lax.all_to_all(pair.astype(jnp.bfloat16), 'x', 0, 0, tiled=True)  17.5 us
    all_gather x1, blocking collectives, body(): q = lax.all_gather(q, 'y')  12.6 us
    pallas_call x1, Pallas kernels, mix(): pl.pallas_call(mix_kernel, in_specs=[pl.BlockSpec(memory_space=pltpu.SMEM...  10.2 us
    pallas_call x1, Pallas kernels, feed(): pl.pallas_call(feed_kernel, in_specs=[pl.BlockSpec(memory_space=pltpu.SME...  9.6 us
    ppermute x2, waiting for transfers between devices, mirrored(): return lax.ppermute(value, 'z', [(i, size - 1 - i) for i in range(size)])  8.8 us
  transfers between devices with their start and end apart: 24, of which 13 were waited for; matrix products, arithmetic and copies ran while one was open for 3% of the time, Pallas kernels for 24%

profile of v1, /device:TPU:1, one launch (start us, length us, event | category | flops | bytes accessed | tf_op | source)
XLA Modules:
  0.0 214.2 jit_solution(8196631528588550771)
XLA Ops:
  6.5 0.8 fusion.2
  7.3 1.8 fusion
  9.2 1.0 fusion.3
  10.2 3.6 %collective-permute-start.18 = (bf16[64,2048]{1,0:T(8,128)(2,1)S(1)}, bf16[64,2048]{1,0:T(8,128)(2,1)S(1)}, u32[]{:S(2)}, u32[]{:S(2)}) collective-permute-start(bf16[64,2048]{1,0:T(8,128)(2,1)S(1)} %get-tuple-element.28), channel_id=1, source_target_pairs={{0,24},{8,0},{16,8},{24,16},{1,25},{9,1},{17,9},{25,17},{2,26},{10... | collective-permute-start | bytes 786440 | tf_op jit(solution)/shard_map/ppermute | solution.py:29
  14.2 0.7 collective-permute-start.16
  14.9 9.4 %collective-permute-done.18 = bf16[64,2048]{1,0:T(8,128)(2,1)S(1)} collective-permute-done((bf16[64,2048]{1,0:T(8,128)(2,1)S(1)}, bf16[64,2048]{1,0:T(8,128)(2,1)S(1)}, u32[]{:S(2)}, u32[]{:S(2)}) %collective-permute-start.18) | collective-permute-done | bytes 262176 | tf_op jit(solution)/shard_map/ppermute | solution.py:29
  24.3 5.0 %collective-permute-done.16 = bf16[64,2048]{1,0:T(8,128)(2,1)S(1)} collective-permute-done((bf16[64,2048]{1,0:T(8,128)(2,1)S(1)}, bf16[64,2048]{1,0:T(8,128)(2,1)S(1)}, u32[]{:S(2)}, u32[]{:S(2)}) %collective-permute-start.16) | collective-permute-done | bytes 262176 | tf_op jit(solution)/shard_map/ppermute | solution.py:29
  29.3 1.1 pad_maximum_fusion
  30.6 1.3 collective-permute-start.1
  31.9 2.5 %collective-permute-start.2 = (bf16[256,2048]{1,0:T(8,128)(2,1)S(1)}, bf16[256,2048]{1,0:T(8,128)(2,1)}, u32[]{:S(2)}, u32[]{:S(2)}) collective-permute-start(bf16[256,2048]{1,0:T(8,128)(2,1)S(1)} %constant_dynamic-update-slice_fusion.refs_0_), channel_id=1, source_target_pairs={{0,4},{2,6},{4,0},{6,2},{1,5},{3,7},{5,1},{7,3},{8,12},{10,14},{12... | collective-permute-start | bytes 3145736 | tf_op jit(solution)/shard_map/ppermute | solution.py:29
  34.4 1.2 collective-permute-start.3
  35.7 5.7 %collective-permute-start = (bf16[256,192]{1,0:T(8,128)(2,1)S(1)}, bf16[256,192]{1,0:T(8,128)(2,1)S(1)}, u32[]{:S(2)}, u32[]{:S(2)}) collective-permute-start(bf16[256,192]{1,0:T(8,128)(2,1)S(1)} %get-tuple-element.30), channel_id=1, source_target_pairs={{0,224},{32,192},{64,160},{96,128},{128,96},{160,64},{192,32},{224... | collective-permute-start | bytes 294920 | tf_op jit(solution)/shard_map/ppermute | solution.py:34
  41.4 0.7 pad_add_fusion.1.at_ref
  42.0 0.6 pad_add_fusion.2.at_ref
  42.6 8.2 %collective-permute-done = bf16[256,192]{1,0:T(8,128)(2,1)S(1)} collective-permute-done((bf16[256,192]{1,0:T(8,128)(2,1)S(1)}, bf16[256,192]{1,0:T(8,128)(2,1)S(1)}, u32[]{:S(2)}, u32[]{:S(2)}) %collective-permute-start) | collective-permute-done | bytes 98336 | tf_op jit(solution)/shard_map/ppermute | solution.py:34
  50.9 12.6 %all-gather = bf16[2048,192]{1,0:T(8,128)(2,1)} all-gather(bf16[512,192]{1,0:T(8,128)(2,1)S(1)} %pad_maximum_fusion.2), channel_id=2, replica_groups=mesh['z'=8,'y'=4,'x'=4,'c'=2] {'y'}, dimensions={0}, use_global_device_ids=true | all-gather | bytes 983040 | tf_op jit(solution)/shard_map/all_gather | solution.py:348
  63.5 8.3 %shard_map.154 = bf16[4,416,256]{2,1,0:T(8,128)(2,1)} custom-call(s32[3]{0:T(128)} %pad_add_fusion.1.at_ref, bf16[4,512,192]{2,1,0:T(8,128)(2,1)} %bitcast.37, bf16[8,768,256]{2,1,0:T(8,128)(2,1)} %bitcast.50), custom_call_target="tpu_custom_call" | custom-call | flops 10000000000 | bytes 6000000 | tf_op jit(solution)/shard_map/pallas_call | solution.py:119
  71.8 3.7 %all-to-all-start = ((bf16[4,416,256]{2,1,0:T(8,128)(2,1)}), bf16[4,416,256]{2,1,0:T(8,128)(2,1)S(1)}, u32[]{:S(2)}, u32[]{:S(2)}) async-start(bf16[4,416,256]{2,1,0:T(8,128)(2,1)} %shard_map.154), calls=%async_computation | async-start | bytes 1703936 | tf_op jit(solution)/shard_map/all_to_all | solution.py:356
  75.5 30.1 %shard_map.155 = bf16[4,416,256]{2,1,0:T(8,128)(2,1)} custom-call(s32[3]{0:T(128)} %pad_add_fusion.2.at_ref, bf16[4,512,192]{2,1,0:T(8,128)(2,1)} %bitcast.38, bf16[8,768,256]{2,1,0:T(8,128)(2,1)} %bitcast.51), custom_call_target="tpu_custom_call" | custom-call | flops 10000000000 | bytes 6000000 | tf_op jit(solution)/shard_map/pallas_call | solution.py:119
  105.7 3.5 %all-to-all-start.1 = ((bf16[4,416,256]{2,1,0:T(8,128)(2,1)}), bf16[4,416,256]{2,1,0:T(8,128)(2,1)S(1)}, u32[]{:S(2)}, u32[]{:S(2)}) async-start(bf16[4,416,256]{2,1,0:T(8,128)(2,1)} %shard_map.155), calls=%async_computation.1 | async-start | bytes 1703936 | tf_op jit(solution)/shard_map/all_to_all | solution.py:360
  110.5 0.7 copy.21.gain_major
  111.2 0.7 copy.22.gain_minor
  111.9 0.7 pad_maximum_fusion.5.lam_ref
  112.6 4.6 %collective-permute-start.12 = (bf16[256,2048]{1,0:T(8,128)(2,1)S(1)}, bf16[256,2048]{1,0:T(8,128)(2,1)}, u32[]{:S(2)}, u32[]{:S(2)}) collective-permute-start(bf16[256,2048]{1,0:T(8,128)(2,1)S(1)} %constant_dynamic-update-slice_fusion.refs_0_), channel_id=1, source_target_pairs={{0,1},{1,0},{2,3},{3,2},{4,5},{5,4},{6,7},{7,6},{8,9},{9,8},{10,11... | collective-permute-start | bytes 3145736 | tf_op jit(solution)/shard_map/ppermute | solution.py:29
  117.9 0.9 copy-done.1
  118.8 2.9 %merge.1 = (bf16[384,128]{1,0:T(8,128)(2,1)}, bf16[384,128]{1,0:T(8,128)(2,1)}) custom-call(s32[1]{0:T(128)} %bitcast.3.first_ref, f32[2]{0:T(128)} %pad_maximum_fusion.5.lam_ref, f32[128,1]{1,0:T(8,128)} %copy.21.gain_major, f32[64,1]{1,0:T(8,128)} %copy.22.gain_minor, bf16[4,416,256]{2,1,0:T(8,128)(2,1)} %copy-done, bf16[4,416,256]{2,1,0:T(8,128)(2,1)} %copy-done.1), custom_call_target="tpu_custom_call" | custom-call | tf_op jit(solution)/shard_map/merge/pallas_call | solution.py:190
  121.7 1.1 collective-permute-start.4
  122.8 0.9 bitcast_dynamic-update-slice_fusion.7
  123.7 4.1 %collective-permute-start.5 = (bf16[384,128]{1,0:T(8,128)(2,1)}, bf16[384,128]{1,0:T(8,128)(2,1)S(1)}, u32[]{:S(2)}, u32[]{:S(2)}) collective-permute-start(bf16[384,128]{1,0:T(8,128)(2,1)} %get-tuple-element.17), channel_id=1, source_target_pairs={{0,4},{2,6},{4,0},{6,2},{1,5},{3,7},{5,1},{7,3},{8,12},{10,14},{12... | collective-permute-start | bytes 294920 | tf_op jit(solution)/shard_map/ppermute | solution.py:29
  128.3 1.5 collective-permute-start.6
  130.6 1.7 collective-permute-done.6
  132.4 5.9 %collective-permute-start.15 = (bf16[256,2048]{1,0:T(8,128)(2,1)}, bf16[256,2048]{1,0:T(8,128)(2,1)}, u32[]{:S(2)}, u32[]{:S(2)}) collective-permute-start(bf16[256,2048]{1,0:T(8,128)(2,1)} %collective-permute-done.3.refs_3_), channel_id=1, source_target_pairs={{0,1},{1,0},{2,3},{3,2},{4,5},{5,4},{6,7},{7,6},{8,9},{9,8},{10,11... | collective-permute-start | bytes 3145736 | tf_op jit(solution)/shard_map/ppermute | solution.py:29
  138.8 1.7 collective-permute-start.8
  140.6 3.3 %collective-permute-done.8 = bf16[384,128]{1,0:T(8,128)(2,1)S(1)} collective-permute-done((bf16[384,128]{1,0:T(8,128)(2,1)S(1)}, bf16[384,128]{1,0:T(8,128)(2,1)S(1)}, u32[]{:S(2)}, u32[]{:S(2)}) %collective-permute-start.8) | collective-permute-done | bytes 98336 | tf_op jit(solution)/shard_map/ppermute | solution.py:29
  143.9 2.5 %collective-permute-start.9 = (bf16[384,128]{1,0:T(8,128)(2,1)S(1)}, bf16[384,128]{1,0:T(8,128)(2,1)S(1)}, u32[]{:S(2)}, u32[]{:S(2)}) collective-permute-start(bf16[384,128]{1,0:T(8,128)(2,1)S(1)} %collective-permute-done.7), channel_id=1, source_target_pairs={{0,4},{2,6},{4,0},{6,2},{1,5},{3,7},{5,1},{7,3},{8,12},{10,14},{12... | collective-permute-start | bytes 294920 | tf_op jit(solution)/shard_map/ppermute | solution.py:29
  146.4 2.6 %collective-permute-done.9 = bf16[384,128]{1,0:T(8,128)(2,1)S(1)} collective-permute-done((bf16[384,128]{1,0:T(8,128)(2,1)S(1)}, bf16[384,128]{1,0:T(8,128)(2,1)S(1)}, u32[]{:S(2)}, u32[]{:S(2)}) %collective-permute-start.9) | collective-permute-done | bytes 98336 | tf_op jit(solution)/shard_map/ppermute | solution.py:29
  149.0 1.2 collective-permute-start.10
  150.3 2.6 %collective-permute-done.10 = bf16[384,128]{1,0:T(8,128)(2,1)S(1)} collective-permute-done((bf16[384,128]{1,0:T(8,128)(2,1)S(1)}, bf16[384,128]{1,0:T(8,128)(2,1)S(1)}, u32[]{:S(2)}, u32[]{:S(2)}) %collective-permute-start.10) | collective-permute-done | bytes 98336 | tf_op jit(solution)/shard_map/ppermute | solution.py:29
  152.9 8.8 %collective-permute-start.11 = (bf16[8,384,128]{2,1,0:T(8,128)(2,1)S(1)}, bf16[8,384,128]{2,1,0:T(8,128)(2,1)S(1)}, u32[]{:S(2)}, u32[]{:S(2)}) collective-permute-start(bf16[8,384,128]{2,1,0:T(8,128)(2,1)S(1)} %bitcast_dynamic-update-slice_fusion.heads0), channel_id=1, source_target_pairs={{0,1},{1,0},{2,3},{3,2},{4,5},{5,4},{6,7},{7,6},{8,9},{9,8},{10,11... | collective-permute-start | bytes 2359304 | tf_op jit(solution)/shard_map/ppermute | solution.py:29
  161.7 0.6 pad_add_fusion.at_ref
  162.3 1.3 collective-permute-done.11.heads1
  163.6 0.9 copy-done.12
  164.5 10.2 %mix.1 = (f32[64,2048]{1,0:T(8,128)}, bf16[512,2048]{1,0:T(8,128)(2,1)}) custom-call(s32[3]{0:T(128)} %pad_add_fusion.at_ref, bf16[8,384,128]{2,1,0:T(8,128)(2,1)} %copy-done.9, bf16[8,384,128]{2,1,0:T(8,128)(2,1)} %copy-done.12, f32[1,2048]{1,0:T(1,128)} %bitcast.52, bf16[256,2048]{1,0:T(8,128)(2,1)} %copy-done.4, ...), custom_call_target="tpu_custom_call" | custom-call | flops 3300000000 | bytes 12000000 | tf_op jit(solution)/shard_map/mix/pallas_call | solution.py:241
  174.7 9.6 %feed.1 = (bf16[4,64,2048]{2,1,0:T(8,128)(2,1)}, bf16[4,64,2048]{2,1,0:T(8,128)(2,1)}) custom-call(s32[3]{0:T(128)} %pad_add_fusion.at_ref, bf16[512,2048]{1,0:T(8,128)(2,1)} %get-tuple-element.24.normed, bf16[8,4,64,2048]{3,2,1,0:T(8,128)(2,1)} %bitcast.49), custom_call_target="tpu_custom_call" | custom-call | flops 4400000000 | bytes 14000000 | tf_op jit(solution)/shard_map/feed/pallas_call | solution.py:298
  184.8 2.5 %collective-permute-done.19 = bf16[4,64,2048]{2,1,0:T(8,128)(2,1)S(1)} collective-permute-done((bf16[4,64,2048]{2,1,0:T(8,128)(2,1)}, bf16[4,64,2048]{2,1,0:T(8,128)(2,1)S(1)}, u32[]{:S(2)}, u32[]{:S(2)}) %collective-permute-start.19) | collective-permute-done | bytes 1048608 | tf_op jit(solution)/shard_map/ppermute | solution.py:29
  187.3 1.6 add_convert_fusion
  188.9 17.5 %all_to_all.15 = bf16[4,64,2048]{2,1,0:T(8,128)(2,1)S(1)} all-to-all(bf16[4,64,2048]{2,1,0:T(8,128)(2,1)S(1)} %add_convert_fusion), channel_id=1, replica_groups=mesh['z'=8,'y'=4,'x'=4,'c'=2] {'x'}, dimensions={0} | all-to-all | bytes 2097152 | tf_op jit(solution)/shard_map/all_to_all | solution.py:369
  206.6 0.8 add_convert_fusion.1
  (62 shorter events, 4.1 us)
Async XLA Ops:
  6.5 57.0 %all-gather.6.cloned.1.call-start = ((), (), s32[]{:S(2)}) async-start(), calls=%async_computation.3 | async-start | bytes 3538944 | tf_op jit(solution)/shard_map/all_gather | solution.py:341
  9.1 21.4 %copy-start.2 = (bf16[128,2048]{1,0:T(8,128)(2,1)S(1)}, bf16[128,2048]{1,0:T(8,128)(2,1)}, u32[]{:S(2)}) copy-start(bf16[128,2048]{1,0:T(8,128)(2,1)} %param.27) | copy-start | bytes 1572868
  9.1 165.6 %all-gather.8.cloned.1.call-start = ((), (), s32[]{:S(2)}) async-start(), calls=%async_computation.4 | async-start | bytes 9437184 | tf_op jit(solution)/shard_map/all_gather | solution.py:351
  10.2 14.1 %collective-permute-start.18 = (bf16[64,2048]{1,0:T(8,128)(2,1)S(1)}, bf16[64,2048]{1,0:T(8,128)(2,1)S(1)}, u32[]{:S(2)}, u32[]{:S(2)}) collective-permute-start(bf16[64,2048]{1,0:T(8,128)(2,1)S(1)} %get-tuple-element.28), channel_id=1, source_target_pairs={{0,24},{8,0},{16,8},{24,16},{1,25},{9,1},{17,9},{25,17},{2,26},{10... | collective-permute-start | bytes 786440 | tf_op jit(solution)/shard_map/ppermute | solution.py:29
  13.9 10.5 %collective-permute-start.17 = (bf16[64,2048]{1,0:T(8,128)(2,1)S(1)}, bf16[64,2048]{1,0:T(8,128)(2,1)S(1)}, u32[]{:S(2)}, u32[]{:S(2)}) collective-permute-start(bf16[64,2048]{1,0:T(8,128)(2,1)S(1)} %get-tuple-element.28), channel_id=1, source_target_pairs={{0,16},{8,24},{16,0},{24,8},{1,17},{9,25},{17,1},{25,9},{2,18},{10... | collective-permute-start | bytes 786440 | tf_op jit(solution)/shard_map/ppermute | solution.py:29
  14.2 15.1 %collective-permute-start.16 = (bf16[64,2048]{1,0:T(8,128)(2,1)S(1)}, bf16[64,2048]{1,0:T(8,128)(2,1)S(1)}, u32[]{:S(2)}, u32[]{:S(2)}) collective-permute-start(bf16[64,2048]{1,0:T(8,128)(2,1)S(1)} %get-tuple-element.28), channel_id=1, source_target_pairs={{0,8},{8,16},{16,24},{24,0},{1,9},{9,17},{17,25},{25,1},{2,10},{10... | collective-permute-start | bytes 786440 | tf_op jit(solution)/shard_map/ppermute | solution.py:29
  29.3 1.2 copy-start.5
  29.3 1.3 copy-start.6
  30.5 5.1 %copy-start.8 = (bf16[512,64]{0,1:T(8,128)(2,1)S(1)}, bf16[512,64]{0,1:T(8,128)(2,1)}, u32[]{:S(2)}) copy-start(bf16[512,64]{0,1:T(8,128)(2,1)} %param.20) | copy-start | bytes 196612
  30.5 5.2 %copy-start.7 = (bf16[512,128]{1,0:T(8,128)(2,1)S(1)}, bf16[512,128]{1,0:T(8,128)(2,1)}, u32[]{:S(2)}) copy-start(bf16[512,128]{1,0:T(8,128)(2,1)} %param.17) | copy-start | bytes 393220
  30.6 81.9 %copy-start.4 = (bf16[256,2048]{1,0:T(8,128)(2,1)}, bf16[256,2048]{1,0:T(8,128)(2,1)S(1)}, u32[]{:S(2)}) copy-start(bf16[256,2048]{1,0:T(8,128)(2,1)S(1)} %constant_dynamic-update-slice_fusion.refs_0_) | copy-start | bytes 3145732
  30.6 75.0 %collective-permute-start.1 = (bf16[256,2048]{1,0:T(8,128)(2,1)S(1)}, bf16[256,2048]{1,0:T(8,128)(2,1)}, u32[]{:S(2)}, u32[]{:S(2)}) collective-permute-start(bf16[256,2048]{1,0:T(8,128)(2,1)S(1)} %constant_dynamic-update-slice_fusion.refs_0_), channel_id=1, source_target_pairs={{0,2},{2,4},{4,6},{6,0},{1,3},{3,5},{5,7},{7,1},{8,10},{10,12},{12... | collective-permute-start | bytes 3145736 | tf_op jit(solution)/shard_map/ppermute | solution.py:29
  31.9 73.7 %collective-permute-start.2 = (bf16[256,2048]{1,0:T(8,128)(2,1)S(1)}, bf16[256,2048]{1,0:T(8,128)(2,1)}, u32[]{:S(2)}, u32[]{:S(2)}) collective-permute-start(bf16[256,2048]{1,0:T(8,128)(2,1)S(1)} %constant_dynamic-update-slice_fusion.refs_0_), channel_id=1, source_target_pairs={{0,4},{2,6},{4,0},{6,2},{1,5},{3,7},{5,1},{7,3},{8,12},{10,14},{12... | collective-permute-start | bytes 3145736 | tf_op jit(solution)/shard_map/ppermute | solution.py:29
  34.4 71.3 %collective-permute-start.3 = (bf16[256,2048]{1,0:T(8,128)(2,1)S(1)}, bf16[256,2048]{1,0:T(8,128)(2,1)}, u32[]{:S(2)}, u32[]{:S(2)}) collective-permute-start(bf16[256,2048]{1,0:T(8,128)(2,1)S(1)} %constant_dynamic-update-slice_fusion.refs_0_), channel_id=1, source_target_pairs={{0,6},{2,0},{4,2},{6,4},{1,7},{3,1},{5,3},{7,5},{8,14},{10,8},{12,... | collective-permute-start | bytes 3145736 | tf_op jit(solution)/shard_map/ppermute | solution.py:29
  35.7 15.1 %collective-permute-start = (bf16[256,192]{1,0:T(8,128)(2,1)S(1)}, bf16[256,192]{1,0:T(8,128)(2,1)S(1)}, u32[]{:S(2)}, u32[]{:S(2)}) collective-permute-start(bf16[256,192]{1,0:T(8,128)(2,1)S(1)} %get-tuple-element.30), channel_id=1, source_target_pairs={{0,224},{32,192},{64,160},{96,128},{128,96},{160,64},{192,32},{224... | collective-permute-start | bytes 294920 | tf_op jit(solution)/shard_map/ppermute | solution.py:34
  71.8 33.8 %all-to-all-start = ((bf16[4,416,256]{2,1,0:T(8,128)(2,1)}), bf16[4,416,256]{2,1,0:T(8,128)(2,1)S(1)}, u32[]{:S(2)}, u32[]{:S(2)}) async-start(bf16[4,416,256]{2,1,0:T(8,128)(2,1)} %shard_map.154), calls=%async_computation | async-start | bytes 1703936 | tf_op jit(solution)/shard_map/all_to_all | solution.py:356
  75.5 35.0 %copy-start.10 = (f32[128]{0:T(128)S(1)}, f32[128]{0:T(128)}, u32[]{:S(2)}) copy-start(f32[128]{0:T(128)} %param.25) | copy-start | bytes 1540
  75.5 35.7 %copy-start.11 = (f32[64]{0:T(128)S(1)}, f32[64]{0:T(128)}, u32[]{:S(2)}) copy-start(f32[64]{0:T(128)} %param.26) | copy-start | bytes 772
  105.7 12.2 %copy-start = (bf16[4,416,256]{2,1,0:T(8,128)(2,1)}, bf16[4,416,256]{2,1,0:T(8,128)(2,1)S(1)}, u32[]{:S(2)}) copy-start(bf16[4,416,256]{2,1,0:T(8,128)(2,1)S(1)} %all-to-all-done.short_ref) | copy-start | bytes 2555908
  105.7 12.2 %all-to-all-start.1 = ((bf16[4,416,256]{2,1,0:T(8,128)(2,1)}), bf16[4,416,256]{2,1,0:T(8,128)(2,1)S(1)}, u32[]{:S(2)}, u32[]{:S(2)}) async-start(bf16[4,416,256]{2,1,0:T(8,128)(2,1)} %shard_map.155), calls=%async_computation.1 | async-start | bytes 1703936 | tf_op jit(solution)/shard_map/all_to_all | solution.py:360
  112.6 49.7 %collective-permute-start.12 = (bf16[256,2048]{1,0:T(8,128)(2,1)S(1)}, bf16[256,2048]{1,0:T(8,128)(2,1)}, u32[]{:S(2)}, u32[]{:S(2)}) collective-permute-start(bf16[256,2048]{1,0:T(8,128)(2,1)S(1)} %constant_dynamic-update-slice_fusion.refs_0_), channel_id=1, source_target_pairs={{0,1},{1,0},{2,3},{3,2},{4,5},{5,4},{6,7},{7,6},{8,9},{9,8},{10,11... | collective-permute-start | bytes 3145736 | tf_op jit(solution)/shard_map/ppermute | solution.py:29
  117.2 45.1 %collective-permute-start.13 = (bf16[256,2048]{1,0:T(8,128)(2,1)}, bf16[256,2048]{1,0:T(8,128)(2,1)}, u32[]{:S(2)}, u32[]{:S(2)}) collective-permute-start(bf16[256,2048]{1,0:T(8,128)(2,1)} %collective-permute-done.1.refs_1_), channel_id=1, source_target_pairs={{0,1},{1,0},{2,3},{3,2},{4,5},{5,4},{6,7},{7,6},{8,9},{9,8},{10,11... | collective-permute-start | bytes 3145736 | tf_op jit(solution)/shard_map/ppermute | solution.py:29
  117.2 45.1 %collective-permute-start.14 = (bf16[256,2048]{1,0:T(8,128)(2,1)}, bf16[256,2048]{1,0:T(8,128)(2,1)}, u32[]{:S(2)}, u32[]{:S(2)}) collective-permute-start(bf16[256,2048]{1,0:T(8,128)(2,1)} %collective-permute-done.2.refs_2_), channel_id=1, source_target_pairs={{0,1},{1,0},{2,3},{3,2},{4,5},{5,4},{6,7},{7,6},{8,9},{9,8},{10,11... | collective-permute-start | bytes 3145736 | tf_op jit(solution)/shard_map/ppermute | solution.py:29
  117.9 0.9 copy-start.1
  121.7 6.6 %collective-permute-start.4 = (bf16[384,128]{1,0:T(8,128)(2,1)}, bf16[384,128]{1,0:T(8,128)(2,1)S(1)}, u32[]{:S(2)}, u32[]{:S(2)}) collective-permute-start(bf16[384,128]{1,0:T(8,128)(2,1)} %get-tuple-element.17), channel_id=1, source_target_pairs={{0,2},{2,4},{4,6},{6,0},{1,3},{3,5},{5,7},{7,1},{8,10},{10,12},{12... | collective-permute-start | bytes 294920 | tf_op jit(solution)/shard_map/ppermute | solution.py:29
  123.7 6.6 %collective-permute-start.5 = (bf16[384,128]{1,0:T(8,128)(2,1)}, bf16[384,128]{1,0:T(8,128)(2,1)S(1)}, u32[]{:S(2)}, u32[]{:S(2)}) collective-permute-start(bf16[384,128]{1,0:T(8,128)(2,1)} %get-tuple-element.17), channel_id=1, source_target_pairs={{0,4},{2,6},{4,0},{6,2},{1,5},{3,7},{5,1},{7,3},{8,12},{10,14},{12... | collective-permute-start | bytes 294920 | tf_op jit(solution)/shard_map/ppermute | solution.py:29
  128.3 4.1 %collective-permute-start.6 = (bf16[384,128]{1,0:T(8,128)(2,1)}, bf16[384,128]{1,0:T(8,128)(2,1)S(1)}, u32[]{:S(2)}, u32[]{:S(2)}) collective-permute-start(bf16[384,128]{1,0:T(8,128)(2,1)} %get-tuple-element.17), channel_id=1, source_target_pairs={{0,6},{2,0},{4,2},{6,4},{1,7},{3,1},{5,3},{7,5},{8,14},{10,8},{12,... | collective-permute-start | bytes 294920 | tf_op jit(solution)/shard_map/ppermute | solution.py:29
  130.3 8.6 %collective-permute-start.7 = (bf16[384,128]{1,0:T(8,128)(2,1)}, bf16[384,128]{1,0:T(8,128)(2,1)S(1)}, u32[]{:S(2)}, u32[]{:S(2)}) collective-permute-start(bf16[384,128]{1,0:T(8,128)(2,1)} %get-tuple-element.18), channel_id=1, source_target_pairs={{0,224},{32,192},{64,160},{96,128},{128,96},{160,64},{192,32},{224... | collective-permute-start | bytes 294920 | tf_op jit(solution)/shard_map/ppermute | solution.py:34
  132.4 30.0 %collective-permute-start.15 = (bf16[256,2048]{1,0:T(8,128)(2,1)}, bf16[256,2048]{1,0:T(8,128)(2,1)}, u32[]{:S(2)}, u32[]{:S(2)}) collective-permute-start(bf16[256,2048]{1,0:T(8,128)(2,1)} %collective-permute-done.3.refs_3_), channel_id=1, source_target_pairs={{0,1},{1,0},{2,3},{3,2},{4,5},{5,4},{6,7},{7,6},{8,9},{9,8},{10,11... | collective-permute-start | bytes 3145736 | tf_op jit(solution)/shard_map/ppermute | solution.py:29
  138.8 5.1 %collective-permute-start.8 = (bf16[384,128]{1,0:T(8,128)(2,1)S(1)}, bf16[384,128]{1,0:T(8,128)(2,1)S(1)}, u32[]{:S(2)}, u32[]{:S(2)}) collective-permute-start(bf16[384,128]{1,0:T(8,128)(2,1)S(1)} %collective-permute-done.7), channel_id=1, source_target_pairs={{0,2},{2,4},{4,6},{6,0},{1,3},{3,5},{5,7},{7,1},{8,10},{10,12},{12... | collective-permute-start | bytes 294920 | tf_op jit(solution)/shard_map/ppermute | solution.py:29
  143.9 5.1 %collective-permute-start.9 = (bf16[384,128]{1,0:T(8,128)(2,1)S(1)}, bf16[384,128]{1,0:T(8,128)(2,1)S(1)}, u32[]{:S(2)}, u32[]{:S(2)}) collective-permute-start(bf16[384,128]{1,0:T(8,128)(2,1)S(1)} %collective-permute-done.7), channel_id=1, source_target_pairs={{0,4},{2,6},{4,0},{6,2},{1,5},{3,7},{5,1},{7,3},{8,12},{10,14},{12... | collective-permute-start | bytes 294920 | tf_op jit(solution)/shard_map/ppermute | solution.py:29
  149.0 3.9 %collective-permute-start.10 = (bf16[384,128]{1,0:T(8,128)(2,1)S(1)}, bf16[384,128]{1,0:T(8,128)(2,1)S(1)}, u32[]{:S(2)}, u32[]{:S(2)}) collective-permute-start(bf16[384,128]{1,0:T(8,128)(2,1)S(1)} %collective-permute-done.7), channel_id=1, source_target_pairs={{0,6},{2,0},{4,2},{6,4},{1,7},{3,1},{5,3},{7,5},{8,14},{10,8},{12,... | collective-permute-start | bytes 294920 | tf_op jit(solution)/shard_map/ppermute | solution.py:29
  152.9 10.7 %copy-start.9 = (bf16[8,384,128]{2,1,0:T(8,128)(2,1)}, bf16[8,384,128]{2,1,0:T(8,128)(2,1)S(1)}, u32[]{:S(2)}) copy-start(bf16[8,384,128]{2,1,0:T(8,128)(2,1)S(1)} %bitcast_dynamic-update-slice_fusion.heads0) | copy-start | bytes 2359300
  152.9 10.7 %collective-permute-start.11 = (bf16[8,384,128]{2,1,0:T(8,128)(2,1)S(1)}, bf16[8,384,128]{2,1,0:T(8,128)(2,1)S(1)}, u32[]{:S(2)}, u32[]{:S(2)}) collective-permute-start(bf16[8,384,128]{2,1,0:T(8,128)(2,1)S(1)} %bitcast_dynamic-update-slice_fusion.heads0), channel_id=1, source_target_pairs={{0,1},{1,0},{2,3},{3,2},{4,5},{5,4},{6,7},{7,6},{8,9},{9,8},{10,11... | collective-permute-start | bytes 2359304 | tf_op jit(solution)/shard_map/ppermute | solution.py:29
  163.6 0.9 copy-start.12
  184.3 3.0 %collective-permute-start.19 = (bf16[4,64,2048]{2,1,0:T(8,128)(2,1)}, bf16[4,64,2048]{2,1,0:T(8,128)(2,1)S(1)}, u32[]{:S(2)}, u32[]{:S(2)}) collective-permute-start(bf16[4,64,2048]{2,1,0:T(8,128)(2,1)} %get-tuple-element.26), channel_id=1, source_target_pairs={{0,1},{1,0},{2,3},{3,2},{4,5},{5,4},{6,7},{7,6},{8,9},{9,8},{10,11... | collective-permute-start | bytes 3145736 | tf_op jit(solution)/shard_map/ppermute | solution.py:29
  188.9 17.7 %copy-start.3 = (f32[64,2048]{1,0:T(8,128)S(1)}, f32[64,2048]{1,0:T(8,128)}, u32[]{:S(2)}) copy-start(f32[64,2048]{1,0:T(8,128)} %get-tuple-element.23) | copy-start | bytes 1572868
Sparse Core Ops, SparseCore 0:
  9.3 53.8 all-gather.5
  64.9 97.3 all-gather.7

commit v2 on v1

--- a/solution.py
+++ b/solution.py
@@ -225,12 +225,10 @@
             x[at + 128 : at + 256, columns] = heads[h * 4 + d, 256:, 64:]
     for copy in copies:
         copy.wait()
-    for h in range(2):
-        at = slice(h * 256, (h + 1) * 256)
-        value = dot(x[at, :], w[...]) + residual[at, :].astype(jnp.float32)
-        stream[at, :] = value
-        mean = jnp.mean(value * value, axis=1, keepdims=True)
-        normed_ref[at, :] = (value * lax.rsqrt(mean + EPSILON) * gain_ref[...]).astype(jnp.bfloat16)
+    value = dot(x[...], w[...]) + residual[...].astype(jnp.float32)
+    stream[...] = value
+    mean = jnp.mean(value * value, axis=1, keepdims=True)
+    normed_ref[...] = (value * lax.rsqrt(mean + EPSILON) * gain_ref[...]).astype(jnp.bfloat16)
     own = pl.ds(pl.multiple_of((own_x * 2 + own_c) * 64, 64), 64)
     stream_ref[...] = stream[own, :]
 
@@ -275,18 +273,19 @@
         copy.start()
     for copy in copies[0]:
         copy.wait()
+    whole = jnp.maximum(dot(normed[...], up[...].reshape(rows, width)), 0.0)
+    whole = (whole * whole).astype(jnp.bfloat16)
     for h in range(2):
-        value = jnp.maximum(dot(normed[h * 256 : (h + 1) * 256, :], up[...].reshape(rows, width)), 0.0)
-        value = (value * value).astype(jnp.bfloat16)
+        value = whole[h * 256 : (h + 1) * 256]
         for k in range(4):
             x, c = h * 2 + k // 2, k % 2
             target = (own_c + c) % 2 * 256 + x * 64
             hidden[pl.ds(pl.multiple_of(target, 64), 64), :] = value[k * 64 : (k + 1) * 64]
     for copy in copies[1]:
         copy.wait()
-    for side, ref in enumerate((keep_ref, send_ref)):
-        out = dot(hidden[side * 256 : (side + 1) * 256, :], down[...].reshape(rows, width), NT)
-        ref[...] = out.astype(jnp.bfloat16).reshape(ref.shape)
+    out = dot(hidden[...], down[...].reshape(rows, width), NT).astype(jnp.bfloat16)
+    keep_ref[...] = out[:256].reshape(keep_ref.shape)
+    send_ref[...] = out[256:].reshape(send_ref.shape)
 
 
 def feed(at, normed, weights):

time: 215 us -> 215 us (level)
  no operation moved by 1% of the time
where the time goes in v2:
time: 215 us; the launch traced here: 214 us
  Pallas kernels  61.4 us (29%)
  starting transfers between devices  55.2 us (26%)
  waiting for transfers between devices  38.5 us (18%)
  blocking collectives  30.1 us (14%)
  between operations  15 us (7%)
  other arithmetic  9.88 us (5%)
  local copies, waits for them, and re-layouts  4.51 us (2%)
    ppermute x18, starting transfers between devices, shifted(): lax.ppermute(value, axis, [(i, (i + by) % size) for i in range(size)])  41.9 us
    pallas_call x2, Pallas kernels, attend(): pl.pallas_call(attend_kernel, grid_spec=pltpu.PrefetchScalarGridSpec(num_...  38.4 us
    ppermute x18, waiting for transfers between devices, shifted(): lax.ppermute(value, axis, [(i, (i + by) % size) for i in range(size)])  29.5 us
    all_to_all x1, blocking collectives, body(): blocks = lax.all_to_all(pair.astype(jnp.bfloat16), 'x', 0, 0, tiled=True)  17.5 us
    all_gather x1, blocking collectives, body(): q = lax.all_gather(q, 'y')  12.6 us
    pallas_call x1, Pallas kernels, mix(): pl.pallas_call(mix_kernel, in_specs=[pl.BlockSpec(memory_space=pltpu.SMEM...  10.2 us
    pallas_call x1, Pallas kernels, feed(): pl.pallas_call(feed_kernel, in_specs=[pl.BlockSpec(memory_space=pltpu.SME...  9.91 us
    ppermute x2, waiting for transfers between devices, mirrored(): return lax.ppermute(value, 'z', [(i, size - 1 - i) for i in range(size)])  8.8 us
  transfers between devices with their start and end apart: 24, of which 13 were waited for; matrix products, arithmetic and copies ran while one was open for 3% of the time, Pallas kernels for 24%

profile of v2, /device:TPU:1, one launch (start us, length us, event | category | flops | bytes accessed | tf_op | source)
XLA Modules:
  0.0 214.5 jit_solution(5179787704761702240)
XLA Ops:
  6.5 0.8 fusion.2
  7.3 1.8 fusion
  9.2 1.0 fusion.3
  10.2 3.6 %collective-permute-start.18 = (bf16[64,2048]{1,0:T(8,128)(2,1)S(1)}, bf16[64,2048]{1,0:T(8,128)(2,1)S(1)}, u32[]{:S(2)}, u32[]{:S(2)}) collective-permute-start(bf16[64,2048]{1,0:T(8,128)(2,1)S(1)} %get-tuple-element.28), channel_id=1, source_target_pairs={{0,24},{8,0},{16,8},{24,16},{1,25},{9,1},{17,9},{25,17},{2,26},{10... | collective-permute-start | bytes 786440 | tf_op jit(solution)/shard_map/ppermute | solution.py:29
  14.2 0.7 collective-permute-start.16
  14.9 9.4 %collective-permute-done.18 = bf16[64,2048]{1,0:T(8,128)(2,1)S(1)} collective-permute-done((bf16[64,2048]{1,0:T(8,128)(2,1)S(1)}, bf16[64,2048]{1,0:T(8,128)(2,1)S(1)}, u32[]{:S(2)}, u32[]{:S(2)}) %collective-permute-start.18) | collective-permute-done | bytes 262176 | tf_op jit(solution)/shard_map/ppermute | solution.py:29
  24.3 5.0 %collective-permute-done.16 = bf16[64,2048]{1,0:T(8,128)(2,1)S(1)} collective-permute-done((bf16[64,2048]{1,0:T(8,128)(2,1)S(1)}, bf16[64,2048]{1,0:T(8,128)(2,1)S(1)}, u32[]{:S(2)}, u32[]{:S(2)}) %collective-permute-start.16) | collective-permute-done | bytes 262176 | tf_op jit(solution)/shard_map/ppermute | solution.py:29
  29.3 1.1 pad_maximum_fusion
  30.6 1.3 collective-permute-start.1
  31.9 2.5 %collective-permute-start.2 = (bf16[256,2048]{1,0:T(8,128)(2,1)S(1)}, bf16[256,2048]{1,0:T(8,128)(2,1)}, u32[]{:S(2)}, u32[]{:S(2)}) collective-permute-start(bf16[256,2048]{1,0:T(8,128)(2,1)S(1)} %constant_dynamic-update-slice_fusion.refs_0_), channel_id=1, source_target_pairs={{0,4},{2,6},{4,0},{6,2},{1,5},{3,7},{5,1},{7,3},{8,12},{10,14},{12... | collective-permute-start | bytes 3145736 | tf_op jit(solution)/shard_map/ppermute | solution.py:29
  34.4 1.2 collective-permute-start.3
  35.7 5.7 %collective-permute-start = (bf16[256,192]{1,0:T(8,128)(2,1)S(1)}, bf16[256,192]{1,0:T(8,128)(2,1)S(1)}, u32[]{:S(2)}, u32[]{:S(2)}) collective-permute-start(bf16[256,192]{1,0:T(8,128)(2,1)S(1)} %get-tuple-element.30), channel_id=1, source_target_pairs={{0,224},{32,192},{64,160},{96,128},{128,96},{160,64},{192,32},{224... | collective-permute-start | bytes 294920 | tf_op jit(solution)/shard_map/ppermute | solution.py:34
  41.4 0.7 pad_add_fusion.1.at_ref
  42.0 0.6 pad_add_fusion.2.at_ref
  42.6 8.2 %collective-permute-done = bf16[256,192]{1,0:T(8,128)(2,1)S(1)} collective-permute-done((bf16[256,192]{1,0:T(8,128)(2,1)S(1)}, bf16[256,192]{1,0:T(8,128)(2,1)S(1)}, u32[]{:S(2)}, u32[]{:S(2)}) %collective-permute-start) | collective-permute-done | bytes 98336 | tf_op jit(solution)/shard_map/ppermute | solution.py:34
  50.9 12.6 %all-gather = bf16[2048,192]{1,0:T(8,128)(2,1)} all-gather(bf16[512,192]{1,0:T(8,128)(2,1)S(1)} %pad_maximum_fusion.2), channel_id=2, replica_groups=mesh['z'=8,'y'=4,'x'=4,'c'=2] {'y'}, dimensions={0}, use_global_device_ids=true | all-gather | bytes 983040 | tf_op jit(solution)/shard_map/all_gather | solution.py:347
  63.5 8.3 %shard_map.154 = bf16[4,416,256]{2,1,0:T(8,128)(2,1)} custom-call(s32[3]{0:T(128)} %pad_add_fusion.1.at_ref, bf16[4,512,192]{2,1,0:T(8,128)(2,1)} %bitcast.37, bf16[8,768,256]{2,1,0:T(8,128)(2,1)} %bitcast.50), custom_call_target="tpu_custom_call" | custom-call | flops 10000000000 | bytes 6000000 | tf_op jit(solution)/shard_map/pallas_call | solution.py:119
  71.8 3.7 %all-to-all-start = ((bf16[4,416,256]{2,1,0:T(8,128)(2,1)}), bf16[4,416,256]{2,1,0:T(8,128)(2,1)S(1)}, u32[]{:S(2)}, u32[]{:S(2)}) async-start(bf16[4,416,256]{2,1,0:T(8,128)(2,1)} %shard_map.154), calls=%async_computation | async-start | bytes 1703936 | tf_op jit(solution)/shard_map/all_to_all | solution.py:355
  75.5 30.1 %shard_map.155 = bf16[4,416,256]{2,1,0:T(8,128)(2,1)} custom-call(s32[3]{0:T(128)} %pad_add_fusion.2.at_ref, bf16[4,512,192]{2,1,0:T(8,128)(2,1)} %bitcast.38, bf16[8,768,256]{2,1,0:T(8,128)(2,1)} %bitcast.51), custom_call_target="tpu_custom_call" | custom-call | flops 10000000000 | bytes 6000000 | tf_op jit(solution)/shard_map/pallas_call | solution.py:119
  105.7 3.5 %all-to-all-start.1 = ((bf16[4,416,256]{2,1,0:T(8,128)(2,1)}), bf16[4,416,256]{2,1,0:T(8,128)(2,1)S(1)}, u32[]{:S(2)}, u32[]{:S(2)}) async-start(bf16[4,416,256]{2,1,0:T(8,128)(2,1)} %shard_map.155), calls=%async_computation.1 | async-start | bytes 1703936 | tf_op jit(solution)/shard_map/all_to_all | solution.py:359
  110.5 0.7 copy.21.gain_major
  111.2 0.7 copy.22.gain_minor
  111.9 0.7 pad_maximum_fusion.5.lam_ref
  112.6 4.6 %collective-permute-start.12 = (bf16[256,2048]{1,0:T(8,128)(2,1)S(1)}, bf16[256,2048]{1,0:T(8,128)(2,1)}, u32[]{:S(2)}, u32[]{:S(2)}) collective-permute-start(bf16[256,2048]{1,0:T(8,128)(2,1)S(1)} %constant_dynamic-update-slice_fusion.refs_0_), channel_id=1, source_target_pairs={{0,1},{1,0},{2,3},{3,2},{4,5},{5,4},{6,7},{7,6},{8,9},{9,8},{10,11... | collective-permute-start | bytes 3145736 | tf_op jit(solution)/shard_map/ppermute | solution.py:29
  117.9 0.9 copy-done.1
  118.8 2.9 %merge.1 = (bf16[384,128]{1,0:T(8,128)(2,1)}, bf16[384,128]{1,0:T(8,128)(2,1)}) custom-call(s32[1]{0:T(128)} %bitcast.3.first_ref, f32[2]{0:T(128)} %pad_maximum_fusion.5.lam_ref, f32[128,1]{1,0:T(8,128)} %copy.21.gain_major, f32[64,1]{1,0:T(8,128)} %copy.22.gain_minor, bf16[4,416,256]{2,1,0:T(8,128)(2,1)} %copy-done, bf16[4,416,256]{2,1,0:T(8,128)(2,1)} %copy-done.1), custom_call_target="tpu_custom_call" | custom-call | tf_op jit(solution)/shard_map/merge/pallas_call | solution.py:190
  121.7 1.1 collective-permute-start.4
  122.8 0.9 bitcast_dynamic-update-slice_fusion.7
  123.7 4.1 %collective-permute-start.5 = (bf16[384,128]{1,0:T(8,128)(2,1)}, bf16[384,128]{1,0:T(8,128)(2,1)S(1)}, u32[]{:S(2)}, u32[]{:S(2)}) collective-permute-start(bf16[384,128]{1,0:T(8,128)(2,1)} %get-tuple-element.17), channel_id=1, source_target_pairs={{0,4},{2,6},{4,0},{6,2},{1,5},{3,7},{5,1},{7,3},{8,12},{10,14},{12... | collective-permute-start | bytes 294920 | tf_op jit(solution)/shard_map/ppermute | solution.py:29
  128.3 1.5 collective-permute-start.6
  130.6 1.7 collective-permute-done.6
  132.4 5.9 %collective-permute-start.15 = (bf16[256,2048]{1,0:T(8,128)(2,1)}, bf16[256,2048]{1,0:T(8,128)(2,1)}, u32[]{:S(2)}, u32[]{:S(2)}) collective-permute-start(bf16[256,2048]{1,0:T(8,128)(2,1)} %collective-permute-done.3.refs_3_), channel_id=1, source_target_pairs={{0,1},{1,0},{2,3},{3,2},{4,5},{5,4},{6,7},{7,6},{8,9},{9,8},{10,11... | collective-permute-start | bytes 3145736 | tf_op jit(solution)/shard_map/ppermute | solution.py:29
  138.8 1.7 collective-permute-start.8
  140.6 3.3 %collective-permute-done.8 = bf16[384,128]{1,0:T(8,128)(2,1)S(1)} collective-permute-done((bf16[384,128]{1,0:T(8,128)(2,1)S(1)}, bf16[384,128]{1,0:T(8,128)(2,1)S(1)}, u32[]{:S(2)}, u32[]{:S(2)}) %collective-permute-start.8) | collective-permute-done | bytes 98336 | tf_op jit(solution)/shard_map/ppermute | solution.py:29
  143.9 2.5 %collective-permute-start.9 = (bf16[384,128]{1,0:T(8,128)(2,1)S(1)}, bf16[384,128]{1,0:T(8,128)(2,1)S(1)}, u32[]{:S(2)}, u32[]{:S(2)}) collective-permute-start(bf16[384,128]{1,0:T(8,128)(2,1)S(1)} %collective-permute-done.7), channel_id=1, source_target_pairs={{0,4},{2,6},{4,0},{6,2},{1,5},{3,7},{5,1},{7,3},{8,12},{10,14},{12... | collective-permute-start | bytes 294920 | tf_op jit(solution)/shard_map/ppermute | solution.py:29
  146.4 2.6 %collective-permute-done.9 = bf16[384,128]{1,0:T(8,128)(2,1)S(1)} collective-permute-done((bf16[384,128]{1,0:T(8,128)(2,1)S(1)}, bf16[384,128]{1,0:T(8,128)(2,1)S(1)}, u32[]{:S(2)}, u32[]{:S(2)}) %collective-permute-start.9) | collective-permute-done | bytes 98336 | tf_op jit(solution)/shard_map/ppermute | solution.py:29
  149.0 1.2 collective-permute-start.10
  150.3 2.6 %collective-permute-done.10 = bf16[384,128]{1,0:T(8,128)(2,1)S(1)} collective-permute-done((bf16[384,128]{1,0:T(8,128)(2,1)S(1)}, bf16[384,128]{1,0:T(8,128)(2,1)S(1)}, u32[]{:S(2)}, u32[]{:S(2)}) %collective-permute-start.10) | collective-permute-done | bytes 98336 | tf_op jit(solution)/shard_map/ppermute | solution.py:29
  152.9 8.8 %collective-permute-start.11 = (bf16[8,384,128]{2,1,0:T(8,128)(2,1)S(1)}, bf16[8,384,128]{2,1,0:T(8,128)(2,1)S(1)}, u32[]{:S(2)}, u32[]{:S(2)}) collective-permute-start(bf16[8,384,128]{2,1,0:T(8,128)(2,1)S(1)} %bitcast_dynamic-update-slice_fusion.heads0), channel_id=1, source_target_pairs={{0,1},{1,0},{2,3},{3,2},{4,5},{5,4},{6,7},{7,6},{8,9},{9,8},{10,11... | collective-permute-start | bytes 2359304 | tf_op jit(solution)/shard_map/ppermute | solution.py:29
  161.7 0.6 pad_add_fusion.at_ref
  162.3 1.3 collective-permute-done.11.heads1
  163.6 0.9 copy-done.12
  164.5 10.2 %mix.1 = (f32[64,2048]{1,0:T(8,128)}, bf16[512,2048]{1,0:T(8,128)(2,1)}) custom-call(s32[3]{0:T(128)} %pad_add_fusion.at_ref, bf16[8,384,128]{2,1,0:T(8,128)(2,1)} %copy-done.9, bf16[8,384,128]{2,1,0:T(8,128)(2,1)} %copy-done.12, f32[1,2048]{1,0:T(1,128)} %bitcast.52, bf16[256,2048]{1,0:T(8,128)(2,1)} %copy-done.4, ...), custom_call_target="tpu_custom_call" | custom-call | flops 3300000000 | bytes 12000000 | tf_op jit(solution)/shard_map/mix/pallas_call | solution.py:239
  174.7 9.9 %feed.1 = (bf16[4,64,2048]{2,1,0:T(8,128)(2,1)}, bf16[4,64,2048]{2,1,0:T(8,128)(2,1)}) custom-call(s32[3]{0:T(128)} %pad_add_fusion.at_ref, bf16[512,2048]{1,0:T(8,128)(2,1)} %get-tuple-element.24.normed, bf16[8,4,64,2048]{3,2,1,0:T(8,128)(2,1)} %bitcast.49), custom_call_target="tpu_custom_call" | custom-call | flops 4400000000 | bytes 14000000 | tf_op jit(solution)/shard_map/feed/pallas_call | solution.py:297
  185.1 2.5 %collective-permute-done.19 = bf16[4,64,2048]{2,1,0:T(8,128)(2,1)S(1)} collective-permute-done((bf16[4,64,2048]{2,1,0:T(8,128)(2,1)}, bf16[4,64,2048]{2,1,0:T(8,128)(2,1)S(1)}, u32[]{:S(2)}, u32[]{:S(2)}) %collective-permute-start.19) | collective-permute-done | bytes 1048608 | tf_op jit(solution)/shard_map/ppermute | solution.py:29
  187.6 1.6 add_convert_fusion
  189.2 17.5 %all_to_all.15 = bf16[4,64,2048]{2,1,0:T(8,128)(2,1)S(1)} all-to-all(bf16[4,64,2048]{2,1,0:T(8,128)(2,1)S(1)} %add_convert_fusion), channel_id=1, replica_groups=mesh['z'=8,'y'=4,'x'=4,'c'=2] {'x'}, dimensions={0} | all-to-all | bytes 2097152 | tf_op jit(solution)/shard_map/all_to_all | solution.py:368
  206.9 0.8 add_convert_fusion.1
  (62 shorter events, 4.1 us)
Async XLA Ops:
  6.5 57.0 %all-gather.6.cloned.1.call-start = ((), (), s32[]{:S(2)}) async-start(), calls=%async_computation.3 | async-start | bytes 3538944 | tf_op jit(solution)/shard_map/all_gather | solution.py:340
  9.1 21.4 %copy-start.2 = (bf16[128,2048]{1,0:T(8,128)(2,1)S(1)}, bf16[128,2048]{1,0:T(8,128)(2,1)}, u32[]{:S(2)}) copy-start(bf16[128,2048]{1,0:T(8,128)(2,1)} %param.27) | copy-start | bytes 1572868
  9.1 165.6 %all-gather.8.cloned.1.call-start = ((), (), s32[]{:S(2)}) async-start(), calls=%async_computation.4 | async-start | bytes 9437184 | tf_op jit(solution)/shard_map/all_gather | solution.py:350
  10.2 14.1 %collective-permute-start.18 = (bf16[64,2048]{1,0:T(8,128)(2,1)S(1)}, bf16[64,2048]{1,0:T(8,128)(2,1)S(1)}, u32[]{:S(2)}, u32[]{:S(2)}) collective-permute-start(bf16[64,2048]{1,0:T(8,128)(2,1)S(1)} %get-tuple-element.28), channel_id=1, source_target_pairs={{0,24},{8,0},{16,8},{24,16},{1,25},{9,1},{17,9},{25,17},{2,26},{10... | collective-permute-start | bytes 786440 | tf_op jit(solution)/shard_map/ppermute | solution.py:29
  13.9 10.5 %collective-permute-start.17 = (bf16[64,2048]{1,0:T(8,128)(2,1)S(1)}, bf16[64,2048]{1,0:T(8,128)(2,1)S(1)}, u32[]{:S(2)}, u32[]{:S(2)}) collective-permute-start(bf16[64,2048]{1,0:T(8,128)(2,1)S(1)} %get-tuple-element.28), channel_id=1, source_target_pairs={{0,16},{8,24},{16,0},{24,8},{1,17},{9,25},{17,1},{25,9},{2,18},{10... | collective-permute-start | bytes 786440 | tf_op jit(solution)/shard_map/ppermute | solution.py:29
  14.2 15.1 %collective-permute-start.16 = (bf16[64,2048]{1,0:T(8,128)(2,1)S(1)}, bf16[64,2048]{1,0:T(8,128)(2,1)S(1)}, u32[]{:S(2)}, u32[]{:S(2)}) collective-permute-start(bf16[64,2048]{1,0:T(8,128)(2,1)S(1)} %get-tuple-element.28), channel_id=1, source_target_pairs={{0,8},{8,16},{16,24},{24,0},{1,9},{9,17},{17,25},{25,1},{2,10},{10... | collective-permute-start | bytes 786440 | tf_op jit(solution)/shard_map/ppermute | solution.py:29
  29.3 1.2 copy-start.5
  29.3 1.3 copy-start.6
  30.5 5.1 %copy-start.8 = (bf16[512,64]{0,1:T(8,128)(2,1)S(1)}, bf16[512,64]{0,1:T(8,128)(2,1)}, u32[]{:S(2)}) copy-start(bf16[512,64]{0,1:T(8,128)(2,1)} %param.20) | copy-start | bytes 196612
  30.5 5.2 %copy-start.7 = (bf16[512,128]{1,0:T(8,128)(2,1)S(1)}, bf16[512,128]{1,0:T(8,128)(2,1)}, u32[]{:S(2)}) copy-start(bf16[512,128]{1,0:T(8,128)(2,1)} %param.17) | copy-start | bytes 393220
  30.6 81.9 %copy-start.4 = (bf16[256,2048]{1,0:T(8,128)(2,1)}, bf16[256,2048]{1,0:T(8,128)(2,1)S(1)}, u32[]{:S(2)}) copy-start(bf16[256,2048]{1,0:T(8,128)(2,1)S(1)} %constant_dynamic-update-slice_fusion.refs_0_) | copy-start | bytes 3145732
  30.6 75.0 %collective-permute-start.1 = (bf16[256,2048]{1,0:T(8,128)(2,1)S(1)}, bf16[256,2048]{1,0:T(8,128)(2,1)}, u32[]{:S(2)}, u32[]{:S(2)}) collective-permute-start(bf16[256,2048]{1,0:T(8,128)(2,1)S(1)} %constant_dynamic-update-slice_fusion.refs_0_), channel_id=1, source_target_pairs={{0,2},{2,4},{4,6},{6,0},{1,3},{3,5},{5,7},{7,1},{8,10},{10,12},{12... | collective-permute-start | bytes 3145736 | tf_op jit(solution)/shard_map/ppermute | solution.py:29
  31.9 73.7 %collective-permute-start.2 = (bf16[256,2048]{1,0:T(8,128)(2,1)S(1)}, bf16[256,2048]{1,0:T(8,128)(2,1)}, u32[]{:S(2)}, u32[]{:S(2)}) collective-permute-start(bf16[256,2048]{1,0:T(8,128)(2,1)S(1)} %constant_dynamic-update-slice_fusion.refs_0_), channel_id=1, source_target_pairs={{0,4},{2,6},{4,0},{6,2},{1,5},{3,7},{5,1},{7,3},{8,12},{10,14},{12... | collective-permute-start | bytes 3145736 | tf_op jit(solution)/shard_map/ppermute | solution.py:29
  34.4 71.3 %collective-permute-start.3 = (bf16[256,2048]{1,0:T(8,128)(2,1)S(1)}, bf16[256,2048]{1,0:T(8,128)(2,1)}, u32[]{:S(2)}, u32[]{:S(2)}) collective-permute-start(bf16[256,2048]{1,0:T(8,128)(2,1)S(1)} %constant_dynamic-update-slice_fusion.refs_0_), channel_id=1, source_target_pairs={{0,6},{2,0},{4,2},{6,4},{1,7},{3,1},{5,3},{7,5},{8,14},{10,8},{12,... | collective-permute-start | bytes 3145736 | tf_op jit(solution)/shard_map/ppermute | solution.py:29
  35.7 15.1 %collective-permute-start = (bf16[256,192]{1,0:T(8,128)(2,1)S(1)}, bf16[256,192]{1,0:T(8,128)(2,1)S(1)}, u32[]{:S(2)}, u32[]{:S(2)}) collective-permute-start(bf16[256,192]{1,0:T(8,128)(2,1)S(1)} %get-tuple-element.30), channel_id=1, source_target_pairs={{0,224},{32,192},{64,160},{96,128},{128,96},{160,64},{192,32},{224... | collective-permute-start | bytes 294920 | tf_op jit(solution)/shard_map/ppermute | solution.py:34
  71.8 33.8 %all-to-all-start = ((bf16[4,416,256]{2,1,0:T(8,128)(2,1)}), bf16[4,416,256]{2,1,0:T(8,128)(2,1)S(1)}, u32[]{:S(2)}, u32[]{:S(2)}) async-start(bf16[4,416,256]{2,1,0:T(8,128)(2,1)} %shard_map.154), calls=%async_computation | async-start | bytes 1703936 | tf_op jit(solution)/shard_map/all_to_all | solution.py:355
  75.5 35.0 %copy-start.10 = (f32[128]{0:T(128)S(1)}, f32[128]{0:T(128)}, u32[]{:S(2)}) copy-start(f32[128]{0:T(128)} %param.25) | copy-start | bytes 1540
  75.5 35.7 %copy-start.11 = (f32[64]{0:T(128)S(1)}, f32[64]{0:T(128)}, u32[]{:S(2)}) copy-start(f32[64]{0:T(128)} %param.26) | copy-start | bytes 772
  105.7 12.2 %copy-start = (bf16[4,416,256]{2,1,0:T(8,128)(2,1)}, bf16[4,416,256]{2,1,0:T(8,128)(2,1)S(1)}, u32[]{:S(2)}) copy-start(bf16[4,416,256]{2,1,0:T(8,128)(2,1)S(1)} %all-to-all-done.short_ref) | copy-start | bytes 2555908
  105.7 12.2 %all-to-all-start.1 = ((bf16[4,416,256]{2,1,0:T(8,128)(2,1)}), bf16[4,416,256]{2,1,0:T(8,128)(2,1)S(1)}, u32[]{:S(2)}, u32[]{:S(2)}) async-start(bf16[4,416,256]{2,1,0:T(8,128)(2,1)} %shard_map.155), calls=%async_computation.1 | async-start | bytes 1703936 | tf_op jit(solution)/shard_map/all_to_all | solution.py:359
  112.6 49.7 %collective-permute-start.12 = (bf16[256,2048]{1,0:T(8,128)(2,1)S(1)}, bf16[256,2048]{1,0:T(8,128)(2,1)}, u32[]{:S(2)}, u32[]{:S(2)}) collective-permute-start(bf16[256,2048]{1,0:T(8,128)(2,1)S(1)} %constant_dynamic-update-slice_fusion.refs_0_), channel_id=1, source_target_pairs={{0,1},{1,0},{2,3},{3,2},{4,5},{5,4},{6,7},{7,6},{8,9},{9,8},{10,11... | collective-permute-start | bytes 3145736 | tf_op jit(solution)/shard_map/ppermute | solution.py:29
  117.2 45.1 %collective-permute-start.13 = (bf16[256,2048]{1,0:T(8,128)(2,1)}, bf16[256,2048]{1,0:T(8,128)(2,1)}, u32[]{:S(2)}, u32[]{:S(2)}) collective-permute-start(bf16[256,2048]{1,0:T(8,128)(2,1)} %collective-permute-done.1.refs_1_), channel_id=1, source_target_pairs={{0,1},{1,0},{2,3},{3,2},{4,5},{5,4},{6,7},{7,6},{8,9},{9,8},{10,11... | collective-permute-start | bytes 3145736 | tf_op jit(solution)/shard_map/ppermute | solution.py:29
  117.2 45.1 %collective-permute-start.14 = (bf16[256,2048]{1,0:T(8,128)(2,1)}, bf16[256,2048]{1,0:T(8,128)(2,1)}, u32[]{:S(2)}, u32[]{:S(2)}) collective-permute-start(bf16[256,2048]{1,0:T(8,128)(2,1)} %collective-permute-done.2.refs_2_), channel_id=1, source_target_pairs={{0,1},{1,0},{2,3},{3,2},{4,5},{5,4},{6,7},{7,6},{8,9},{9,8},{10,11... | collective-permute-start | bytes 3145736 | tf_op jit(solution)/shard_map/ppermute | solution.py:29
  117.9 0.9 copy-start.1
  121.7 6.6 %collective-permute-start.4 = (bf16[384,128]{1,0:T(8,128)(2,1)}, bf16[384,128]{1,0:T(8,128)(2,1)S(1)}, u32[]{:S(2)}, u32[]{:S(2)}) collective-permute-start(bf16[384,128]{1,0:T(8,128)(2,1)} %get-tuple-element.17), channel_id=1, source_target_pairs={{0,2},{2,4},{4,6},{6,0},{1,3},{3,5},{5,7},{7,1},{8,10},{10,12},{12... | collective-permute-start | bytes 294920 | tf_op jit(solution)/shard_map/ppermute | solution.py:29
  123.7 6.6 %collective-permute-start.5 = (bf16[384,128]{1,0:T(8,128)(2,1)}, bf16[384,128]{1,0:T(8,128)(2,1)S(1)}, u32[]{:S(2)}, u32[]{:S(2)}) collective-permute-start(bf16[384,128]{1,0:T(8,128)(2,1)} %get-tuple-element.17), channel_id=1, source_target_pairs={{0,4},{2,6},{4,0},{6,2},{1,5},{3,7},{5,1},{7,3},{8,12},{10,14},{12... | collective-permute-start | bytes 294920 | tf_op jit(solution)/shard_map/ppermute | solution.py:29
  128.3 4.1 %collective-permute-start.6 = (bf16[384,128]{1,0:T(8,128)(2,1)}, bf16[384,128]{1,0:T(8,128)(2,1)S(1)}, u32[]{:S(2)}, u32[]{:S(2)}) collective-permute-start(bf16[384,128]{1,0:T(8,128)(2,1)} %get-tuple-element.17), channel_id=1, source_target_pairs={{0,6},{2,0},{4,2},{6,4},{1,7},{3,1},{5,3},{7,5},{8,14},{10,8},{12,... | collective-permute-start | bytes 294920 | tf_op jit(solution)/shard_map/ppermute | solution.py:29
  130.3 8.6 %collective-permute-start.7 = (bf16[384,128]{1,0:T(8,128)(2,1)}, bf16[384,128]{1,0:T(8,128)(2,1)S(1)}, u32[]{:S(2)}, u32[]{:S(2)}) collective-permute-start(bf16[384,128]{1,0:T(8,128)(2,1)} %get-tuple-element.18), channel_id=1, source_target_pairs={{0,224},{32,192},{64,160},{96,128},{128,96},{160,64},{192,32},{224... | collective-permute-start | bytes 294920 | tf_op jit(solution)/shard_map/ppermute | solution.py:34
  132.4 30.0 %collective-permute-start.15 = (bf16[256,2048]{1,0:T(8,128)(2,1)}, bf16[256,2048]{1,0:T(8,128)(2,1)}, u32[]{:S(2)}, u32[]{:S(2)}) collective-permute-start(bf16[256,2048]{1,0:T(8,128)(2,1)} %collective-permute-done.3.refs_3_), channel_id=1, source_target_pairs={{0,1},{1,0},{2,3},{3,2},{4,5},{5,4},{6,7},{7,6},{8,9},{9,8},{10,11... | collective-permute-start | bytes 3145736 | tf_op jit(solution)/shard_map/ppermute | solution.py:29
  138.8 5.1 %collective-permute-start.8 = (bf16[384,128]{1,0:T(8,128)(2,1)S(1)}, bf16[384,128]{1,0:T(8,128)(2,1)S(1)}, u32[]{:S(2)}, u32[]{:S(2)}) collective-permute-start(bf16[384,128]{1,0:T(8,128)(2,1)S(1)} %collective-permute-done.7), channel_id=1, source_target_pairs={{0,2},{2,4},{4,6},{6,0},{1,3},{3,5},{5,7},{7,1},{8,10},{10,12},{12... | collective-permute-start | bytes 294920 | tf_op jit(solution)/shard_map/ppermute | solution.py:29
  143.9 5.1 %collective-permute-start.9 = (bf16[384,128]{1,0:T(8,128)(2,1)S(1)}, bf16[384,128]{1,0:T(8,128)(2,1)S(1)}, u32[]{:S(2)}, u32[]{:S(2)}) collective-permute-start(bf16[384,128]{1,0:T(8,128)(2,1)S(1)} %collective-permute-done.7), channel_id=1, source_target_pairs={{0,4},{2,6},{4,0},{6,2},{1,5},{3,7},{5,1},{7,3},{8,12},{10,14},{12... | collective-permute-start | bytes 294920 | tf_op jit(solution)/shard_map/ppermute | solution.py:29
  149.0 3.9 %collective-permute-start.10 = (bf16[384,128]{1,0:T(8,128)(2,1)S(1)}, bf16[384,128]{1,0:T(8,128)(2,1)S(1)}, u32[]{:S(2)}, u32[]{:S(2)}) collective-permute-start(bf16[384,128]{1,0:T(8,128)(2,1)S(1)} %collective-permute-done.7), channel_id=1, source_target_pairs={{0,6},{2,0},{4,2},{6,4},{1,7},{3,1},{5,3},{7,5},{8,14},{10,8},{12,... | collective-permute-start | bytes 294920 | tf_op jit(solution)/shard_map/ppermute | solution.py:29
  152.9 10.7 %copy-start.9 = (bf16[8,384,128]{2,1,0:T(8,128)(2,1)}, bf16[8,384,128]{2,1,0:T(8,128)(2,1)S(1)}, u32[]{:S(2)}) copy-start(bf16[8,384,128]{2,1,0:T(8,128)(2,1)S(1)} %bitcast_dynamic-update-slice_fusion.heads0) | copy-start | bytes 2359300
  152.9 10.7 %collective-permute-start.11 = (bf16[8,384,128]{2,1,0:T(8,128)(2,1)S(1)}, bf16[8,384,128]{2,1,0:T(8,128)(2,1)S(1)}, u32[]{:S(2)}, u32[]{:S(2)}) collective-permute-start(bf16[8,384,128]{2,1,0:T(8,128)(2,1)S(1)} %bitcast_dynamic-update-slice_fusion.heads0), channel_id=1, source_target_pairs={{0,1},{1,0},{2,3},{3,2},{4,5},{5,4},{6,7},{7,6},{8,9},{9,8},{10,11... | collective-permute-start | bytes 2359304 | tf_op jit(solution)/shard_map/ppermute | solution.py:29
  163.6 0.9 copy-start.12
  184.6 3.0 %collective-permute-start.19 = (bf16[4,64,2048]{2,1,0:T(8,128)(2,1)}, bf16[4,64,2048]{2,1,0:T(8,128)(2,1)S(1)}, u32[]{:S(2)}, u32[]{:S(2)}) collective-permute-start(bf16[4,64,2048]{2,1,0:T(8,128)(2,1)} %get-tuple-element.26), channel_id=1, source_target_pairs={{0,1},{1,0},{2,3},{3,2},{4,5},{5,4},{6,7},{7,6},{8,9},{9,8},{10,11... | collective-permute-start | bytes 3145736 | tf_op jit(solution)/shard_map/ppermute | solution.py:29
  189.2 17.7 %copy-start.3 = (f32[64,2048]{1,0:T(8,128)S(1)}, f32[64,2048]{1,0:T(8,128)}, u32[]{:S(2)}) copy-start(f32[64,2048]{1,0:T(8,128)} %get-tuple-element.23) | copy-start | bytes 1572868
Sparse Core Ops, SparseCore 0:
  9.3 53.8 all-gather.5
  64.9 97.3 all-gather.7
